TPU v7x, 32 devices: a whole 2x2x4 slice. The times are simulated.
32 devices in a mesh: sp: 4 (over z), tp: 8 (over y, x, core).
Axes of the slice: x: 2, y: 2, z: 4, core: 2. Of those that a mesh axis runs over, the one named last changes fastest.
Arguments:
- tokens: bfloat16 [3072, 2048], P('sp'), may hold values from -6 to 6
- norm_gain: float32 [2048], replicated, may hold values from 0.5 to 80
- grid_query_weight: bfloat16 [2048, 2048], P(None, 'tp'), may hold values from -0.5 to 0.5
- grid_key_weight: bfloat16 [2048, 1024], P(None, 'tp'), may hold values from -0.5 to 0.5
- grid_value_weight: bfloat16 [2048, 1024], P(None, 'tp'), may hold values from -0.5 to 0.5
- grid_query_gain: float32 [128], replicated, may hold values from 1.6 to 6
- grid_key_gain: float32 [128], replicated, may hold values from 1.6 to 6
- local_query_weight: bfloat16 [2048, 2048], P(None, 'tp'), may hold values from -0.5 to 0.5
- local_key_weight: bfloat16 [2048, 1024], P(None, 'tp'), may hold values from -0.5 to 0.5
- local_value_weight: bfloat16 [2048, 1024], P(None, 'tp'), may hold values from -0.5 to 0.5
- sink_logit: float32 [16], P('tp'), may hold values from 1 to 6
- grid_out_weight: bfloat16 [2048, 2048], P('tp'), may hold values from -0.09375 to 0.09375
- local_out_weight: bfloat16 [2048, 2048], P('tp'), may hold values from -0.09375 to 0.09375
Outputs:
- mixed: bfloat16 [3072, 2048], P(('sp', 'tp'))
All inputs are finite; a program needn't handle non-finite values.
Results may differ from a plain program's by a relative error of at most 0.03.
Values may be sent and summed in bfloat16 or wider, within the bound.
No kernel may reach another device: no remote copies, remote signals or barrier semaphores. Data moves between devices by JAX's collectives and lax.ppermute only.
A program may use at most 192 MiB of HBM per device.

v0:
```python
import functools
import math

import jax
import jax.numpy as jnp
import numpy as np
from jax import lax
from jax.experimental import pallas as pl
from jax.experimental.pallas import tpu as pltpu
from jax.sharding import PartitionSpec as P


HEAD = 128
WINDOW = 128
GRID_W = 64
EPSILON = 1e-06
ROPE_BASE = 10000.0
MASKED = -1e30
LOG2E = math.log2(math.e)
MIB = 1 << 20
COST = 0.3

bf16 = jnp.bfloat16
f32 = jnp.float32
ROWS_T = (((1,), (1,)), ((), ()))


def dot(a, b):
    return jnp.dot(a, b, preferred_element_type=f32)


def turn_tables(total_rows, seq_devices):
    half = HEAD // 2
    quarter = half // 2
    inverse = (ROPE_BASE ** (-np.arange(0, half, 2, dtype=np.float32) / np.float32(half))).astype(np.float32)

    def tables(count, first):
        angles = np.arange(count, dtype=np.float32)[:, None] * inverse
        out = np.zeros((3, count, HEAD), np.float32)
        base = 0 if first else half
        out[0, :, base : base + quarter] = np.cos(angles)
        out[0, :, base + quarter : base + half] = np.cos(angles)
        out[1, :, base : base + quarter] = -np.sin(angles)
        out[2, :, base + quarter : base + half] = np.sin(angles)
        return out

    rows = tables(total_rows // GRID_W, True)
    rows = rows.reshape(3, seq_devices, -1, HEAD).transpose(1, 0, 2, 3)
    return rows, tables(GRID_W, False)


def norm_turn(part, gain, row_tab, col_tab, first_row, grid_rows):
    x = part.astype(bf16).astype(f32)
    x = x * lax.rsqrt(jnp.mean(x * x, axis=-1, keepdims=True) + EPSILON) * gain

    def table(k):
        rows = row_tab[k, pl.ds(first_row, grid_rows), :]
        return (rows[:, None, :] + col_tab[k][None, :, :]).reshape(grid_rows * GRID_W, HEAD)

    quarter = HEAD // 4
    return (
        x * table(0)
        + pltpu.roll(x, HEAD - quarter, 1) * table(1)
        + pltpu.roll(x, quarter, 1) * table(2)
    )


def place():
    tp = lax.axis_index("tp")
    core, mine = tp % 2, tp // 2
    return lax.axis_index("sp"), core, (mine ^ 3, mine ^ (1 + core), mine ^ (2 - core), mine)


def start_copies(pairs, sems):
    copies = [pltpu.make_async_copy(src, dst, sems.at[i]) for i, (src, dst) in enumerate(pairs)]
    for copy in copies:
        copy.start()
    return copies


def norm_rows(x, gain):
    x = x.astype(f32)
    return (x * lax.rsqrt(jnp.mean(x * x, axis=-1, keepdims=True) + EPSILON) * gain).astype(bf16)


def kv_rows(first_row, normed, wk, wv, kgain, row_tab, col_tab, kv):
    y = dot(normed[...], jnp.concatenate([wk[...], wv[...]], axis=1))
    keys = norm_turn(y[:, :HEAD], kgain[...], row_tab, col_tab, first_row // GRID_W, normed.shape[0] // GRID_W)
    kv[...] = jnp.concatenate([keys, y[:, HEAD:]], axis=1).astype(bf16)


def first_keys_body(tile, tok, gain, kgain, row_tab, col_tab, wk, wv,
                    normed, kv, tok_b, gain_v, kgain_v, row_v, col_v, wk_v, wv_v, tok_v, sems):
    half = normed.shape[0]
    rows = [pl.ds(i, tile) for i in range(0, half, tile)]
    pairs = [(gain, gain_v)] + [(tok.at[r], tok_v.at[r]) for r in rows] + [(wk, wk_v), (wv, wv_v)]
    pairs += [(kgain, kgain_v), (row_tab.at[place()[0]], row_v), (col_tab, col_v)]
    copies = start_copies(pairs + [(tok.at[pl.ds(half, half)], tok_b)], sems)
    copies[0].wait()
    for r, copy in zip(rows, copies[1:]):
        copy.wait()
        normed[r, :] = norm_rows(tok_v[r, :], gain_v[...])
    for copy in copies[1 + len(rows) : -1]:
        copy.wait()
    kv_rows(0, normed, wk_v, wv_v, kgain_v, row_v, col_v, kv)
    copies[-1].wait()


def second_keys_body(tok, gain, kgain, row_tab, col_tab, wk, wv, wq, lwq, lwk, lwv, qgain,
                     normed, kv, wq_v, lwq_v, lwk_v, lwv_v, qgain_v, sems):
    pairs = [(wq, wq_v), (lwq, lwq_v), (lwk, lwk_v), (lwv, lwv_v), (qgain, qgain_v)]
    copies = start_copies(pairs, sems)
    normed[...] = norm_rows(tok[...], gain[...])
    kv_rows(normed.shape[0], normed, wk, wv, kgain, row_tab, col_tab, kv)
    for copy in copies:
        copy.wait()


def q_body(normed_a, normed_b, wq, lwq, lwk, lwv, qgain, row_tab, col_tab, q, lq, lkv, first_edge, last_edge):
    row_count = lq.shape[0]
    tile = row_count // 2
    heads = wq.shape[1] // HEAD
    gain = qgain[...] * (HEAD ** (-0.5) * LOG2E)
    for start, normed in ((0, normed_a), (tile, normed_b)):
        rows = pl.ds(start, tile)
        y = dot(normed[...], jnp.concatenate([wq[...], lwq[...], lwk[...], lwv[...]], axis=1))
        for h in range(heads):
            part = y[:, h * HEAD : (h + 1) * HEAD]
            turned = norm_turn(part, gain, row_tab, col_tab, start // GRID_W, tile // GRID_W)
            q[pl.ds(h * row_count + start, tile), :] = turned.astype(bf16)
        lq[rows, :] = y[:, heads * HEAD : 2 * heads * HEAD].astype(bf16)
        lkv[rows, :] = y[:, 2 * heads * HEAD :].astype(bf16)
    first_edge[...] = lkv[pl.ds(0, WINDOW), :]
    last_edge[...] = lkv[pl.ds(row_count - WINDOW, WINDOW), :]


def split_rows(whole, keep, send):
    piece = keep.shape[0] // (whole.shape[0] // keep.shape[0] * 2)
    count = keep.shape[0] // piece
    core = place()[1]
    for part, flip in ((keep, 0), (send, 1)):
        for i in range(count):
            start = pl.multiple_of(2 * i * piece + (core ^ flip) * piece, 16)
            part[pl.ds(i * piece, piece), :] = whole[pl.ds(start, piece), :]


def local_body(blocks, total_rows, sink, lq, lkv, low, high, keep, send, out):
    offset = place()[0] * (blocks * WINDOW)
    scale = HEAD ** (-0.5) * LOG2E
    heads = lq.shape[1] // HEAD
    shape = (heads * WINDOW, 3 * WINDOW)
    row = lax.broadcasted_iota(jnp.int32, shape, 0) % WINDOW
    col = lax.broadcasted_iota(jnp.int32, shape, 1)
    band = jnp.abs(col - WINDOW - row) <= WINDOW
    bound = jnp.concatenate(
        [jnp.broadcast_to(sink[:, h : h + 1] * LOG2E, (WINDOW, 1)) for h in range(heads)], axis=0
    )
    ones = jnp.ones((3 * WINDOW, HEAD), bf16)
    pieces = [low[...]] + [lkv[pl.ds(i * WINDOW, WINDOW), :] for i in range(blocks)] + [high[...]]
    for i in range(blocks):
        keys = jnp.concatenate([p[:, :HEAD] for p in pieces[i : i + 3]], axis=0)
        values = jnp.concatenate([p[:, HEAD:] for p in pieces[i : i + 3]], axis=0)
        valid = band
        if i == 0 or i == blocks - 1:
            pos = offset + (i - 1) * WINDOW + col
            valid = band & (pos >= 0) & (pos < total_rows)
        rows = pl.ds(i * WINDOW, WINDOW)
        query = jnp.concatenate([lq[rows, h * HEAD : (h + 1) * HEAD] for h in range(heads)], axis=0)
        s = lax.dot_general(query, keys, ROWS_T, preferred_element_type=f32) * scale
        s = jnp.where(valid, s, MASKED)
        top = jnp.maximum(jnp.max(s, axis=-1, keepdims=True), bound)
        p = jnp.exp2(s - top).astype(bf16)
        o = dot(p, jnp.concatenate([values, ones], axis=1))
        o = (o[:, :HEAD] / (o[:, HEAD:] + jnp.exp2(bound - top))).astype(bf16)
        for h in range(heads):
            out[rows, h * HEAD : (h + 1) * HEAD] = o[h * WINDOW : (h + 1) * WINDOW]
    split_rows(out, keep, send)


def softmax_step(query, pairs, m, acc):
    keys = jnp.concatenate([kv[:, :HEAD] for kv in pairs], axis=0)
    values = jnp.concatenate([kv[:, HEAD:] for kv in pairs], axis=0)
    values = jnp.concatenate([values, jnp.ones_like(values)], axis=1)
    s = lax.dot_general(query, keys, ROWS_T, preferred_element_type=f32)
    top = jnp.broadcast_to(jnp.max(s, axis=-1, keepdims=True), (query.shape[0], HEAD))
    new = top if m is None else jnp.maximum(m, top)
    p = jnp.exp2(s - jnp.concatenate([new] * (keys.shape[0] // HEAD), axis=1)).astype(bf16)
    add = dot(p, values)
    if m is not None:
        factor = jnp.exp2(m - new)
        add = acc * jnp.concatenate([factor, factor], axis=1) + add
    return new, add


def attend_body(tile, blocks, first, *refs):
    q = refs[0]
    kvs = refs[1 : 1 + 2 * blocks]
    rest = refs[1 + 2 * blocks :]
    if first:
        w, lw, m_out, acc_out, w_v, lw_v, sems = rest
        copies = start_copies([(w, w_v), (lw, lw_v)], sems)
    else:
        m_out, acc_out = rest[-2:]
    for start in range(0, q.shape[0], tile):
        rows = pl.ds(start, tile)
        m, acc = (None, None) if first else (rest[0][rows, :], rest[1][rows, :])
        for i in range(blocks):
            m, acc = softmax_step(q[rows, :], kvs[2 * i : 2 * i + 2], m, acc)
        m_out[rows, :] = m
        acc_out[rows, :] = acc
    if first:
        for copy in copies:
            copy.wait()


def finish_body(flips, row_count, q, kva, kvb, m_in, acc_in, keep, send):
    _, core, pieces = place()
    piece = keep.shape[0] // len(flips)
    for i, flip in enumerate(flips):
        out_rows = pl.ds(i * piece, piece)
        for h in range(q.shape[0] // row_count):
            start = h * row_count + (pieces[3] ^ flip) * 2 * piece
            rows = pl.ds(pl.multiple_of(start, 16), 2 * piece)
            _, acc = softmax_step(q[rows, :], (kva, kvb), m_in[rows, :], acc_in[rows, :])
            o = acc[:, :HEAD] / acc[:, HEAD:]
            lanes = slice(h * HEAD, (h + 1) * HEAD)
            keep[out_rows, lanes] = jnp.where(core == 0, o[:piece], o[piece:]).astype(bf16)
            send[out_rows, lanes] = jnp.where(core == 0, o[piece:], o[:piece]).astype(bf16)


def project_body(slots, keep, other, lkeep, lother, w, lw, w_other, lw_other, *outs):
    piece = outs[0].shape[-2]
    _, core, pieces = place()
    held = (0, 1 + core, 2 - core, 3)
    weights = jnp.concatenate([w[...], w_other[...], lw[...], lw_other[...]], axis=0)
    for slot, out in zip(slots, outs):
        rows = pl.ds(pl.multiple_of(held[slot] * piece, 16), piece)
        lrows = pl.ds(pl.multiple_of(pieces[slot] * piece, 16), piece)
        part = jnp.concatenate([keep[rows, :], other[rows, :], lkeep[lrows, :], lother[lrows, :]], axis=1)
        out[...] = dot(part, weights).astype(out.dtype)


def vmem(count):
    return [pl.BlockSpec(memory_space=pltpu.VMEM)] * count


def sds(shape, dtype):
    return jax.ShapeDtypeStruct(shape, dtype)


def cost(flops, transcendentals=0, bytes_accessed=0):
    return pl.CostEstimate(flops=int(COST * flops), transcendentals=int(transcendentals), bytes_accessed=int(bytes_accessed))


def hbm(count):
    return [pl.BlockSpec(memory_space=pltpu.HBM)] * count


def in_hbm(*arrays):
    return [pltpu.with_memory_space_constraint(a, pltpu.HBM) for a in arrays]


def params(mib):
    return pltpu.CompilerParams(vmem_limit_bytes=mib * MIB)


def attend(q, blocks, state, bring=()):
    rows = q.shape[0]
    operands = [q] + [part for block in blocks for part in block] + list(state or ())
    keys = sum(part.shape[0] for block in blocks for part in block)
    out_shape = (sds((rows, HEAD), f32), sds((rows, 2 * HEAD), f32)) + tuple(sds(a.shape, a.dtype) for a in bring)
    return pl.pallas_call(
        functools.partial(attend_body, 256, len(blocks), state is None),
        out_shape=out_shape,
        in_specs=vmem(len(operands)) + hbm(len(bring)),
        out_specs=tuple(vmem(len(out_shape))),
        scratch_shapes=[pltpu.SemaphoreType.DMA((len(bring),))] if bring else [],
        compiler_params=params(16),
        cost_estimate=cost(rows * keys * HEAD * 8, rows * keys),
    )(*operands, *in_hbm(*bring))


def finish(q, block, state, flips, row_count, piece):
    rows = q.shape[0]
    keys = 2 * block[0].shape[0]
    done = 2 * piece * len(flips) * rows // row_count
    return pl.pallas_call(
        functools.partial(finish_body, flips, row_count),
        out_shape=(sds((piece * len(flips), rows // row_count * HEAD), bf16),) * 2,
        in_specs=vmem(5),
        out_specs=tuple(vmem(2)),
        compiler_params=params(16),
        cost_estimate=cost(done * keys * HEAD * 8, done * keys),
        name="finish",
    )(q, *block, *state)


def project(slots, operands, piece, dtype):
    width = operands[-1].shape[1]
    depth = 4 * operands[0].shape[1]
    return pl.pallas_call(
        functools.partial(project_body, slots),
        out_shape=tuple(sds((piece, width), dtype) for _ in slots),
        in_specs=vmem(8),
        out_specs=tuple(vmem(len(slots))),
        compiler_params=params(8),
        cost_estimate=cost(2 * piece * width * depth * len(slots), 0, 4 * MIB),
        name="project",
    )(*operands)


def shards(
    tokens,
    norm_gain,
    grid_query_weight,
    grid_key_weight,
    grid_value_weight,
    grid_query_gain,
    grid_key_gain,
    local_query_weight,
    local_key_weight,
    local_value_weight,
    sink_logit,
    grid_out_weight,
    local_out_weight,
):
    row_count, width = tokens.shape
    n_sp = lax.axis_size("sp")
    n_tp = lax.axis_size("tp")
    total_rows = row_count * n_sp
    heads = grid_query_weight.shape[1] // HEAD
    row_np, col_np = turn_tables(total_rows, n_sp)
    row_tab, col_tab = jnp.asarray(row_np), jnp.asarray(col_np)

    tile = 128
    half = row_count // 2
    table_shape = (3, row_count // GRID_W, HEAD)

    tables = (sds((1, width), f32), sds((1, HEAD), f32), sds(table_shape, f32), sds((3, GRID_W, HEAD), f32))
    key_weights = grid_key_weight, grid_value_weight
    query_weights = grid_query_weight, local_query_weight, local_key_weight, local_value_weight
    rows_out = sds((half, width), bf16), sds((half, 2 * HEAD), bf16)
    key_cost = cost(2 * half * width * 2 * HEAD, 0, 4 * MIB)
    normed_a, kva, tokens_b, *shared = pl.pallas_call(
        functools.partial(first_keys_body, tile),
        out_shape=rows_out + (sds((half, width), bf16),) + tables + tuple(sds(w.shape, bf16) for w in key_weights),
        in_specs=hbm(7),
        out_specs=tuple(vmem(9)),
        scratch_shapes=[pltpu.VMEM((half, width), bf16), pltpu.SemaphoreType.DMA((7 + half // tile,))],
        compiler_params=params(16),
        cost_estimate=key_cost,
        name="keys_a",
    )(*in_hbm(tokens, norm_gain.reshape(1, width), grid_key_gain.reshape(1, HEAD), row_tab, col_tab, *key_weights))
    normed_b, kvb, *held = pl.pallas_call(
        second_keys_body,
        out_shape=rows_out + tuple(sds(w.shape, bf16) for w in query_weights) + (sds((1, HEAD), f32),),
        in_specs=vmem(7) + hbm(5),
        out_specs=tuple(vmem(7)),
        scratch_shapes=[pltpu.SemaphoreType.DMA((5,))],
        compiler_params=params(16),
        cost_estimate=key_cost,
        name="keys_b",
    )(tokens_b, *shared, *in_hbm(*query_weights, grid_query_gain.reshape(1, HEAD)))

    forward = [(i, (i + 1) % n_sp) for i in range(n_sp)]
    backward = [(t, s) for s, t in forward]


    def shift(low, high):
        low_a = lax.ppermute(low[0], "sp", forward)
        high_a = lax.ppermute(high[0], "sp", backward)
        low_b = lax.ppermute(low[1], "sp", forward)
        high_b = lax.ppermute(high[1], "sp", backward)
        return (low_a, low_b), (high_a, high_b)

    low, high = shift((kva, kvb), (kva, kvb))

    q, lq, lkv, first_edge, last_edge = pl.pallas_call(
        q_body,
        out_shape=(
            sds((heads * row_count, HEAD), bf16),
            sds((row_count, heads * HEAD), bf16),
            sds((row_count, 2 * HEAD), bf16),
            sds((WINDOW, 2 * HEAD), bf16),
            sds((WINDOW, 2 * HEAD), bf16),
        ),
        in_specs=vmem(9),
        out_specs=tuple(vmem(5)),
        compiler_params=params(16),
        cost_estimate=cost(2 * row_count * width * 6 * HEAD, 0, 6 * MIB),
        name="queries",
    )(normed_a, normed_b, *held, *shared[2:4])

    flip = [(i, i ^ 1) for i in range(n_tp)]
    first_hop = [(i, i ^ (2 + 2 * (i % 2))) for i in range(n_tp)]
    second_hop = [(i, i ^ (4 - 2 * (i % 2))) for i in range(n_tp)]
    low_edge = lax.ppermute(last_edge, "sp", forward[:-1])
    high_edge = lax.ppermute(first_edge, "sp", backward[:-1])
    *state, w_own, lw_own = attend(q, [(kva, kvb), (low[0], high[0])], None, (grid_out_weight, local_out_weight))
    w_other = lax.ppermute(w_own, "tp", flip)
    lw_other = lax.ppermute(lw_own, "tp", flip)
    for _ in range(1, (n_sp - 1) // 2):
        next_low, next_high = shift(low, high)
        state = attend(q, [(low[1], high[1]), (next_low[0], next_high[0])], state)
        low, high = next_low, next_high
    far = lax.ppermute(low[0], "sp", forward), lax.ppermute(high[1], "sp", backward)

    lkeep, lsend = pl.pallas_call(
        functools.partial(local_body, row_count // WINDOW, total_rows),
        out_shape=(sds((row_count // 2, heads * HEAD), bf16),) * 2,
        in_specs=vmem(5),
        out_specs=tuple(vmem(2)),
        scratch_shapes=[pltpu.VMEM((row_count, heads * HEAD), bf16)],
        compiler_params=params(16),
        cost_estimate=cost(heads * row_count * 3 * WINDOW * HEAD * 8, heads * row_count * 3 * WINDOW),
        name="banded",
    )(sink_logit.reshape(1, heads), lq, lkv, low_edge, high_edge)
    lother = lax.ppermute(lsend, "tp", flip)
    state = attend(q, [(low[1], high[1])], state)

    piece = row_count // n_tp
    keep, send = finish(q, far, state, (3, 1, 2, 0), row_count, piece)
    other = lax.ppermute(send, "tp", flip)
    operands = (keep, other, lkeep, lother, w_own, lw_own, w_other, lw_other)
    (pass_on,) = project((0,), operands, piece, bf16)
    got_on = lax.ppermute(pass_on, "tp", first_hop)
    (direct,) = project((1,), operands, piece, bf16)
    got = lax.ppermute(direct, "tp", first_hop)
    next_part, own_part = project((2, 3), operands, piece, f32)
    got_next = lax.ppermute((next_part + got_on.astype(f32)).astype(bf16), "tp", second_hop)
    return (own_part + got.astype(f32) + got_next.astype(f32)).astype(bf16)


def solution(mesh):
    in_specs = (
        P("sp", None),
        P(),
        P(None, "tp"),
        P(None, "tp"),
        P(None, "tp"),
        P(),
        P(),
        P(None, "tp"),
        P(None, "tp"),
        P(None, "tp"),
        P("tp"),
        P("tp", None),
        P("tp", None),
    )
    out_specs = P(("sp", "tp"), None)

    return jax.shard_map(shards, mesh=mesh, in_specs=in_specs, out_specs=out_specs, check_vma=False)
```

profile of v0, /device:TPU:0, one launch (start us, length us, event | category | flops | bytes accessed | tf_op | source)
XLA Modules:
  0.0 66.8 jit_solution(9816061120831108815)
XLA Ops:
  0.0 2.7 %keys_a.1 = (bf16[384,2048]{1,0:T(8,128)(2,1)S(1)}, bf16[384,256]{1,0:T(8,128)(2,1)S(1)}, bf16[384,2048]{1,0:T(8,128)(2,1)S(1)}, f32[1,2048]{1,0:T(1,128)S(1)}, ...) custom-call(bf16[768,2048]{1,0:T(8,128)(2,1)} %tok.1, ...), custom_call_target="tpu_custom_call" | custom-call | flops 120795952 | bytes 4194304 | tf_op jit(solution)/shard_map/keys_a/pallas_call | solution.py:344
  2.7 3.1 %collective-permute-start = (bf16[384,256]{1,0:T(8,128)(2,1)S(1)}, bf16[384,256]{1,0:T(8,128)(2,1)S(1)}, u32[]{:S(2)}, u32[]{:S(2)}) collective-permute-start(bf16[384,256]{1,0:T(8,128)(2,1)S(1)} %get-tuple-element.53.refs_1_), channel_id=1, source_target_pairs={{0,8},{8,16},{16,24},{24,0},{1,9},{9,17},{17,25},{25,1},{2,10},{10... | collective-permute-start | bytes 589832 | tf_op jit(solution)/shard_map/ppermute | solution.py:370
  5.8 2.1 %collective-permute-start.5 = (bf16[384,256]{1,0:T(8,128)(2,1)S(1)}, bf16[384,256]{1,0:T(8,128)(2,1)S(1)}, u32[]{:S(2)}, u32[]{:S(2)}) collective-permute-start(bf16[384,256]{1,0:T(8,128)(2,1)S(1)} %get-tuple-element.53.refs_1_), channel_id=1, source_target_pairs={{8,0},{16,8},{24,16},{0,24},{9,1},{17,9},{25,17},{1,25},{10,2},{18... | collective-permute-start | bytes 589832 | tf_op jit(solution)/shard_map/ppermute | solution.py:371
  7.9 3.0 %keys_b.1 = (bf16[384,2048]{1,0:T(8,128)(2,1)S(1)}, bf16[384,256]{1,0:T(8,128)(2,1)S(1)}, bf16[2048,256]{1,0:T(8,128)(2,1)S(1)}, bf16[2048,256]{1,0:T(8,128)(2,1...) custom-call(bf16[384,2048]{1,0:T(8,128)(2,1)S(1)} %get-tuple-element.39.tok, ...), custom_call_target="tpu_custom_call" | custom-call | flops 120795952 | bytes 4194304 | tf_op jit(solution)/shard_map/keys_b/pallas_call | solution.py:354
  10.9 2.7 %queries.1 = (bf16[1536,128]{1,0:T(8,128)(2,1)S(1)}, bf16[768,256]{1,0:T(8,128)(2,1)S(1)}, bf16[768,256]{1,0:T(8,128)(2,1)S(1)}, bf16[128,256]{1,0:T(8,128)(2,1)S(1)}, bf16[128,256]{1,0:T(8,128)(2,1)S(1)}) custom-call(bf16[384,2048]{1,0:T(8,128)(2,1)S(1)} %get-tuple-element.38.normed_a, bf16[384,2048]{1,0:T(8,128)(2,1)S(1)} %get-tuple-element.46.normed_b, ...), custom_call_target="tpu_custom_call" | custom-call | flops 724775744 | bytes 6291456 | tf_op jit(solution)/shard_map/queries/pallas_call | solution.py:378
  13.6 0.0 collective-permute-done.refs_3_
  13.6 2.7 %collective-permute-done.5.refs_4_ = bf16[384,256]{1,0:T(8,128)(2,1)S(1)} collective-permute-done((bf16[384,256]{1,0:T(8,128)(2,1)S(1)}, bf16[384,256]{1,0:T(8,128)(2,1)S(1)}, u32[]{:S(2)}, u32[]{:S(2)}) %collective-permute-start.5) | collective-permute-done | bytes 196640 | tf_op jit(solution)/shard_map/ppermute | solution.py:371
  16.3 0.0 copy-start
  16.3 3.1 %shard_map.145 = (f32[1536,128]{1,0:T(8,128)S(1)}, f32[1536,256]{1,0:T(8,128)S(1)}, bf16[256,2048]{1,0:T(8,128)(2,1)S(1)}, bf16[256,2048]{1,0:T(8,128)(2,1)S(1)}) custom-call(bf16[1536,128]{1,0:T(8,128)(2,1)S(1)} %get-tuple-element.52.refs_0_.q, bf16[384,256]{1,0:T(8,128)(2,1)S(1)} %get-tuple-element.53.refs_1_, ...), custom_call_target="tpu_custom_call" | custom-call | flops 724775744 | tf_op jit(solution)/shard_map/pallas_call | solution.py:272
  19.4 0.1 collective-permute-start.10
  19.5 0.5 collective-permute-start.11
  20.0 2.3 %collective-permute-start.2 = (bf16[384,256]{1,0:T(8,128)(2,1)S(1)}, bf16[384,256]{1,0:T(8,128)(2,1)S(1)}, u32[]{:S(2)}, u32[]{:S(2)}) collective-permute-start(bf16[384,256]{1,0:T(8,128)(2,1)S(1)} %get-tuple-element.54.refs_2_), channel_id=1, source_target_pairs={{8,0},{16,8},{24,16},{0,24},{9,1},{17,9},{25,17},{1,25},{10,2},{18... | collective-permute-start | bytes 589832 | tf_op jit(solution)/shard_map/ppermute | solution.py:373
  22.3 1.6 %collective-permute-start.7 = (bf16[128,256]{1,0:T(8,128)(2,1)S(1)}, bf16[128,256]{1,0:T(8,128)(2,1)S(1)}, u32[]{:S(2)}, u32[]{:S(2)}) collective-permute-start(bf16[128,256]{1,0:T(8,128)(2,1)S(1)} %get-tuple-element.63), channel_id=1, source_target_pairs={{0,8},{8,16},{16,24},{1,9},{9,17},{17,25},{2,10},{10,18},{18,26},{... | collective-permute-start | bytes 196616 | tf_op jit(solution)/shard_map/ppermute | solution.py:397
  23.9 1.3 %collective-permute-start.8 = (bf16[128,256]{1,0:T(8,128)(2,1)S(1)}, bf16[128,256]{1,0:T(8,128)(2,1)S(1)}, u32[]{:S(2)}, u32[]{:S(2)}) collective-permute-start(bf16[128,256]{1,0:T(8,128)(2,1)S(1)} %get-tuple-element.64), channel_id=1, source_target_pairs={{8,0},{16,8},{24,16},{9,1},{17,9},{25,17},{10,2},{18,10},{26,18},{... | collective-permute-start | bytes 196616 | tf_op jit(solution)/shard_map/ppermute | solution.py:398
  25.2 2.9 %collective-permute-done.7.low = bf16[128,256]{1,0:T(8,128)(2,1)S(1)} collective-permute-done((bf16[128,256]{1,0:T(8,128)(2,1)S(1)}, bf16[128,256]{1,0:T(8,128)(2,1)S(1)}, u32[]{:S(2)}, u32[]{:S(2)}) %collective-permute-start.7) | collective-permute-done | bytes 65568 | tf_op jit(solution)/shard_map/ppermute | solution.py:397
  28.2 2.5 %collective-permute-start.4 = (bf16[384,256]{1,0:T(8,128)(2,1)S(1)}, bf16[384,256]{1,0:T(8,128)(2,1)S(1)}, u32[]{:S(2)}, u32[]{:S(2)}) collective-permute-start(bf16[384,256]{1,0:T(8,128)(2,1)S(1)} %get-tuple-element.54.refs_2_), channel_id=1, source_target_pairs={{0,8},{8,16},{16,24},{24,0},{1,9},{9,17},{17,25},{25,1},{2,10},{10... | collective-permute-start | bytes 589832 | tf_op jit(solution)/shard_map/ppermute | solution.py:372
  30.7 0.0 collective-permute-done.2.refs_2_
  30.7 1.8 %collective-permute-start.3 = (bf16[384,256]{1,0:T(8,128)(2,1)S(1)}, bf16[384,256]{1,0:T(8,128)(2,1)S(1)}, u32[]{:S(2)}, u32[]{:S(2)}) collective-permute-start(bf16[384,256]{1,0:T(8,128)(2,1)S(1)} %collective-permute-done.2.refs_2_), channel_id=1, source_target_pairs={{8,0},{16,8},{24,16},{0,24},{9,1},{17,9},{25,17},{1,25},{10,2},{18... | collective-permute-start | bytes 589832 | tf_op jit(solution)/shard_map/ppermute | solution.py:406
  32.4 0.0 collective-permute-done.8.high
  32.4 0.3 collective-permute-start.1
  32.7 0.0 copy-done
  32.7 2.1 %banded.1 = (bf16[384,256]{1,0:T(8,128)(2,1)S(1)}, bf16[384,256]{1,0:T(8,128)(2,1)S(1)}) custom-call(f32[1,2]{1,0:T(1,128)S(1)} %bitcast.4, bf16[768,256]{1,0:T(8,128)(2,1)S(1)} %get-tuple-element.61.lq, bf16[768,256]{1,0:T(8,128)(2,1)S(1)} %get-tuple-element.62.lkv, bf16[128,256]{1,0:T(8,128)(2,1)S(1)} %collective-permute-done.7.low, ...), custom_call_target="tpu_custom_call" | custom-call | flops 181193936 | tf_op jit(solution)/shard_map/banded/pallas_call | solution.py:408
  34.8 3.4 %collective-permute-done.4.refs_1_ = bf16[384,256]{1,0:T(8,128)(2,1)S(1)} collective-permute-done((bf16[384,256]{1,0:T(8,128)(2,1)S(1)}, bf16[384,256]{1,0:T(8,128)(2,1)S(1)}, u32[]{:S(2)}, u32[]{:S(2)}) %collective-permute-start.4) | collective-permute-done | bytes 196640 | tf_op jit(solution)/shard_map/ppermute | solution.py:372
  38.2 0.0 collective-permute-start.9
  38.2 1.9 %shard_map.146 = (f32[1536,128]{1,0:T(8,128)S(1)}, f32[1536,256]{1,0:T(8,128)S(1)}) custom-call(bf16[1536,128]{1,0:T(8,128)(2,1)S(1)} %get-tuple-element.52.refs_0_.q, bf16[384,256]{1,0:T(8,128)(2,1)S(1)} %collective-permute-done.4.refs_1_, bf16[384,256]{1,0:T(8,128)(2,1)S(1)} %collective-permute-done.2.refs_2_, f32[1536,128]{1,0:T(8,128)S(1)} %get-tuple-element.55.refs_3_, ...), custom_call_target="tpu_custom_call" | custom-call | flops 362387872 | tf_op jit(solution)/shard_map/pallas_call | solution.py:272
  40.1 1.0 %collective-permute-done.3.kvb = bf16[384,256]{1,0:T(8,128)(2,1)S(1)} collective-permute-done((bf16[384,256]{1,0:T(8,128)(2,1)S(1)}, bf16[384,256]{1,0:T(8,128)(2,1)S(1)}, u32[]{:S(2)}, u32[]{:S(2)}) %collective-permute-start.3) | collective-permute-done | bytes 196640 | tf_op jit(solution)/shard_map/ppermute | solution.py:406
  41.1 4.9 %collective-permute-done.1.kva = bf16[384,256]{1,0:T(8,128)(2,1)S(1)} collective-permute-done((bf16[384,256]{1,0:T(8,128)(2,1)S(1)}, bf16[384,256]{1,0:T(8,128)(2,1)S(1)}, u32[]{:S(2)}, u32[]{:S(2)}) %collective-permute-start.1) | collective-permute-done | bytes 196640 | tf_op jit(solution)/shard_map/ppermute | solution.py:406
  46.0 1.9 %finish.1 = (bf16[384,256]{1,0:T(8,128)(2,1)S(1)}, bf16[384,256]{1,0:T(8,128)(2,1)S(1)}) custom-call(bf16[1536,128]{1,0:T(8,128)(2,1)S(1)} %get-tuple-element.52.refs_0_.q, bf16[384,256]{1,0:T(8,128)(2,1)S(1)} %collective-permute-done.1.kva, bf16[384,256]{1,0:T(8,128)(2,1)S(1)} %collective-permute-done.3.kvb, f32[1536,128]{1,0:T(8,128)S(1)} %get-tuple-element.57.m_in, ...), custom_call_target="tpu_custom_call" | custom-call | flops 362387872 | tf_op jit(solution)/shard_map/finish/pallas_call | solution.py:287
  47.8 0.1 collective-permute-start.6
  47.9 0.0 collective-permute-done.9.lother
  47.9 1.4 %collective-permute-done.6.other = bf16[384,256]{1,0:T(8,128)(2,1)S(1)} collective-permute-done((bf16[384,256]{1,0:T(8,128)(2,1)S(1)}, bf16[384,256]{1,0:T(8,128)(2,1)S(1)}, u32[]{:S(2)}, u32[]{:S(2)}) %collective-permute-start.6) | collective-permute-done | bytes 196640 | tf_op jit(solution)/shard_map/ppermute | solution.py:423
  49.3 0.0 collective-permute-done.10.w_other
  49.3 0.0 collective-permute-done.11.lw_other
  49.3 0.8 %project.5 = bf16[96,2048]{1,0:T(8,128)(2,1)S(1)} custom-call(bf16[384,256]{1,0:T(8,128)(2,1)S(1)} %get-tuple-element.59.keep, bf16[384,256]{1,0:T(8,128)(2,1)S(1)} %collective-permute-done.6.other, bf16[384,256]{1,0:T(8,128)(2,1)S(1)} %get-tuple-element.65.lkeep, bf16[384,256]{1,0:T(8,128)(2,1)S(1)} %collective-permute-done.9.lother, ...), custom_call_target="tpu_custom_call" | custom-call | flops 120795952 | bytes 4194304 | tf_op jit(solution)/shard_map/project/pallas_call | solution.py:301
  50.1 1.5 %collective-permute-start.13 = (bf16[96,2048]{1,0:T(8,128)(2,1)S(1)}, bf16[96,2048]{1,0:T(8,128)(2,1)S(1)}, u32[]{:S(2)}, u32[]{:S(2)}) collective-permute-start(bf16[96,2048]{1,0:T(8,128)(2,1)S(1)} %project.5), channel_id=1, source_target_pairs={{0,2},{1,5},{2,0},{3,7},{4,6},{5,1},{6,4},{7,3},{8,10},{9,13},{10,... | collective-permute-start | bytes 1179656 | tf_op jit(solution)/shard_map/ppermute | solution.py:426
  51.7 0.8 %project.4 = bf16[96,2048]{1,0:T(8,128)(2,1)S(1)} custom-call(bf16[384,256]{1,0:T(8,128)(2,1)S(1)} %get-tuple-element.59.keep, bf16[384,256]{1,0:T(8,128)(2,1)S(1)} %collective-permute-done.6.other, bf16[384,256]{1,0:T(8,128)(2,1)S(1)} %get-tuple-element.65.lkeep, bf16[384,256]{1,0:T(8,128)(2,1)S(1)} %collective-permute-done.9.lother, ...), custom_call_target="tpu_custom_call" | custom-call | flops 120795952 | bytes 4194304 | tf_op jit(solution)/shard_map/project/pallas_call | solution.py:301
  52.5 0.6 collective-permute-start.12
  53.1 1.5 %project.3 = (f32[96,2048]{1,0:T(8,128)S(1)}, f32[96,2048]{1,0:T(8,128)S(1)}) custom-call(bf16[384,256]{1,0:T(8,128)(2,1)S(1)} %get-tuple-element.59.keep, bf16[384,256]{1,0:T(8,128)(2,1)S(1)} %collective-permute-done.6.other, bf16[384,256]{1,0:T(8,128)(2,1)S(1)} %get-tuple-element.65.lkeep, bf16[384,256]{1,0:T(8,128)(2,1)S(1)} %collective-permute-done.9.lother, ...), custom_call_target="tpu_custom_call" | custom-call | flops 241591904 | bytes 4194304 | tf_op jit(solution)/shard_map/project/pallas_call | solution.py:301
  54.6 3.4 %collective-permute-done.13 = bf16[96,2048]{1,0:T(8,128)(2,1)S(1)} collective-permute-done((bf16[96,2048]{1,0:T(8,128)(2,1)S(1)}, bf16[96,2048]{1,0:T(8,128)(2,1)S(1)}, u32[]{:S(2)}, u32[]{:S(2)}) %collective-permute-start.13) | collective-permute-done | bytes 393248 | tf_op jit(solution)/shard_map/ppermute | solution.py:426
  58.0 0.1 add_convert_fusion.1
  58.1 1.6 %collective-permute-start.14 = (bf16[96,2048]{1,0:T(8,128)(2,1)S(1)}, bf16[96,2048]{1,0:T(8,128)(2,1)S(1)}, u32[]{:S(2)}, u32[]{:S(2)}) collective-permute-start(bf16[96,2048]{1,0:T(8,128)(2,1)S(1)} %add_convert_fusion.1), channel_id=1, source_target_pairs={{0,4},{1,3},{2,6},{3,1},{4,0},{5,7},{6,2},{7,5},{8,12},{9,11},{10,... | collective-permute-start | bytes 1179656 | tf_op jit(solution)/shard_map/ppermute | solution.py:430
  59.6 4.7 %collective-permute-done.12 = bf16[96,2048]{1,0:T(8,128)(2,1)S(1)} collective-permute-done((bf16[96,2048]{1,0:T(8,128)(2,1)S(1)}, bf16[96,2048]{1,0:T(8,128)(2,1)S(1)}, u32[]{:S(2)}, u32[]{:S(2)}) %collective-permute-start.12) | collective-permute-done | bytes 393248 | tf_op jit(solution)/shard_map/ppermute | solution.py:428
  64.4 1.5 %collective-permute-done.14 = bf16[96,2048]{1,0:T(8,128)(2,1)S(1)} collective-permute-done((bf16[96,2048]{1,0:T(8,128)(2,1)S(1)}, bf16[96,2048]{1,0:T(8,128)(2,1)S(1)}, u32[]{:S(2)}, u32[]{:S(2)}) %collective-permute-start.14) | collective-permute-done | bytes 393248 | tf_op jit(solution)/shard_map/ppermute | solution.py:430
  65.9 0.9 %add_convert_fusion = bf16[96,2048]{1,0:T(8,128)(2,1)} fusion(bf16[96,2048]{1,0:T(8,128)(2,1)S(1)} %collective-permute-done.14, f32[96,2048]{1,0:T(8,128)S(1)} %get-tuple-element.69, bf16[96,2048]{1,0:T(8,128)(2,1)S(1)} %collective-permute-done.12), kind=kLoop, calls=%fused_computation | loop fusion | flops 983040 | bytes 1966080 | tf_op jit(solution)/shard_map/convert_element_type | solution.py:431
Async XLA Ops:
  2.7 11.0 %collective-permute-start = (bf16[384,256]{1,0:T(8,128)(2,1)S(1)}, bf16[384,256]{1,0:T(8,128)(2,1)S(1)}, u32[]{:S(2)}, u32[]{:S(2)}) collective-permute-start(bf16[384,256]{1,0:T(8,128)(2,1)S(1)} %get-tuple-element.53.refs_1_), channel_id=1, source_target_pairs={{0,8},{8,16},{16,24},{24,0},{1,9},{9,17},{17,25},{25,1},{2,10},{10... | collective-permute-start | bytes 589832 | tf_op jit(solution)/shard_map/ppermute | solution.py:370
  5.8 10.6 %collective-permute-start.5 = (bf16[384,256]{1,0:T(8,128)(2,1)S(1)}, bf16[384,256]{1,0:T(8,128)(2,1)S(1)}, u32[]{:S(2)}, u32[]{:S(2)}) collective-permute-start(bf16[384,256]{1,0:T(8,128)(2,1)S(1)} %get-tuple-element.53.refs_1_), channel_id=1, source_target_pairs={{8,0},{16,8},{24,16},{0,24},{9,1},{17,9},{25,17},{1,25},{10,2},{18... | collective-permute-start | bytes 589832 | tf_op jit(solution)/shard_map/ppermute | solution.py:371
  16.3 16.4 %copy-start = (f32[2]{0:T(128)S(1)}, f32[2]{0:T(128)}, u32[]{:S(2)}) copy-start(f32[2]{0:T(128)} %param.25) | copy-start | bytes 28
  19.4 29.9 %collective-permute-start.10 = (bf16[256,2048]{1,0:T(8,128)(2,1)S(1)}, bf16[256,2048]{1,0:T(8,128)(2,1)S(1)}, u32[]{:S(2)}, u32[]{:S(2)}) collective-permute-start(bf16[256,2048]{1,0:T(8,128)(2,1)S(1)} %get-tuple-element.67.w), channel_id=1, source_target_pairs={{0,1},{1,0},{2,3},{3,2},{4,5},{5,4},{6,7},{7,6},{8,9},{9,8},{10,11... | collective-permute-start | bytes 3145736 | tf_op jit(solution)/shard_map/ppermute | solution.py:400
  19.5 29.8 %collective-permute-start.11 = (bf16[256,2048]{1,0:T(8,128)(2,1)S(1)}, bf16[256,2048]{1,0:T(8,128)(2,1)S(1)}, u32[]{:S(2)}, u32[]{:S(2)}) collective-permute-start(bf16[256,2048]{1,0:T(8,128)(2,1)S(1)} %get-tuple-element.68.lw), channel_id=1, source_target_pairs={{0,1},{1,0},{2,3},{3,2},{4,5},{5,4},{6,7},{7,6},{8,9},{9,8},{10,11... | collective-permute-start | bytes 3145736 | tf_op jit(solution)/shard_map/ppermute | solution.py:401
  20.0 10.7 %collective-permute-start.2 = (bf16[384,256]{1,0:T(8,128)(2,1)S(1)}, bf16[384,256]{1,0:T(8,128)(2,1)S(1)}, u32[]{:S(2)}, u32[]{:S(2)}) collective-permute-start(bf16[384,256]{1,0:T(8,128)(2,1)S(1)} %get-tuple-element.54.refs_2_), channel_id=1, source_target_pairs={{8,0},{16,8},{24,16},{0,24},{9,1},{17,9},{25,17},{1,25},{10,2},{18... | collective-permute-start | bytes 589832 | tf_op jit(solution)/shard_map/ppermute | solution.py:373
  22.3 5.9 %collective-permute-start.7 = (bf16[128,256]{1,0:T(8,128)(2,1)S(1)}, bf16[128,256]{1,0:T(8,128)(2,1)S(1)}, u32[]{:S(2)}, u32[]{:S(2)}) collective-permute-start(bf16[128,256]{1,0:T(8,128)(2,1)S(1)} %get-tuple-element.63), channel_id=1, source_target_pairs={{0,8},{8,16},{16,24},{1,9},{9,17},{17,25},{2,10},{10,18},{18,26},{... | collective-permute-start | bytes 196616 | tf_op jit(solution)/shard_map/ppermute | solution.py:397
  23.9 8.5 %collective-permute-start.8 = (bf16[128,256]{1,0:T(8,128)(2,1)S(1)}, bf16[128,256]{1,0:T(8,128)(2,1)S(1)}, u32[]{:S(2)}, u32[]{:S(2)}) collective-permute-start(bf16[128,256]{1,0:T(8,128)(2,1)S(1)} %get-tuple-element.64), channel_id=1, source_target_pairs={{8,0},{16,8},{24,16},{9,1},{17,9},{25,17},{10,2},{18,10},{26,18},{... | collective-permute-start | bytes 196616 | tf_op jit(solution)/shard_map/ppermute | solution.py:398
  28.2 10.0 %collective-permute-start.4 = (bf16[384,256]{1,0:T(8,128)(2,1)S(1)}, bf16[384,256]{1,0:T(8,128)(2,1)S(1)}, u32[]{:S(2)}, u32[]{:S(2)}) collective-permute-start(bf16[384,256]{1,0:T(8,128)(2,1)S(1)} %get-tuple-element.54.refs_2_), channel_id=1, source_target_pairs={{0,8},{8,16},{16,24},{24,0},{1,9},{9,17},{17,25},{25,1},{2,10},{10... | collective-permute-start | bytes 589832 | tf_op jit(solution)/shard_map/ppermute | solution.py:372
  30.7 10.4 %collective-permute-start.3 = (bf16[384,256]{1,0:T(8,128)(2,1)S(1)}, bf16[384,256]{1,0:T(8,128)(2,1)S(1)}, u32[]{:S(2)}, u32[]{:S(2)}) collective-permute-start(bf16[384,256]{1,0:T(8,128)(2,1)S(1)} %collective-permute-done.2.refs_2_), channel_id=1, source_target_pairs={{8,0},{16,8},{24,16},{0,24},{9,1},{17,9},{25,17},{1,25},{10,2},{18... | collective-permute-start | bytes 589832 | tf_op jit(solution)/shard_map/ppermute | solution.py:406
  32.4 13.5 %collective-permute-start.1 = (bf16[384,256]{1,0:T(8,128)(2,1)S(1)}, bf16[384,256]{1,0:T(8,128)(2,1)S(1)}, u32[]{:S(2)}, u32[]{:S(2)}) collective-permute-start(bf16[384,256]{1,0:T(8,128)(2,1)S(1)} %collective-permute-done.refs_3_), channel_id=1, source_target_pairs={{0,8},{8,16},{16,24},{24,0},{1,9},{9,17},{17,25},{25,1},{2,10},{10... | collective-permute-start | bytes 589832 | tf_op jit(solution)/shard_map/ppermute | solution.py:406
  38.2 9.7 %collective-permute-start.9 = (bf16[384,256]{1,0:T(8,128)(2,1)S(1)}, bf16[384,256]{1,0:T(8,128)(2,1)S(1)}, u32[]{:S(2)}, u32[]{:S(2)}) collective-permute-start(bf16[384,256]{1,0:T(8,128)(2,1)S(1)} %get-tuple-element.66), channel_id=1, source_target_pairs={{0,1},{1,0},{2,3},{3,2},{4,5},{5,4},{6,7},{7,6},{8,9},{9,8},{10,11... | collective-permute-start | bytes 589832 | tf_op jit(solution)/shard_map/ppermute | solution.py:418
  47.8 1.5 %collective-permute-start.6 = (bf16[384,256]{1,0:T(8,128)(2,1)S(1)}, bf16[384,256]{1,0:T(8,128)(2,1)S(1)}, u32[]{:S(2)}, u32[]{:S(2)}) collective-permute-start(bf16[384,256]{1,0:T(8,128)(2,1)S(1)} %get-tuple-element.60), channel_id=1, source_target_pairs={{0,1},{1,0},{2,3},{3,2},{4,5},{5,4},{6,7},{7,6},{8,9},{9,8},{10,11... | collective-permute-start | bytes 589832 | tf_op jit(solution)/shard_map/ppermute | solution.py:423
  50.1 7.8 %collective-permute-start.13 = (bf16[96,2048]{1,0:T(8,128)(2,1)S(1)}, bf16[96,2048]{1,0:T(8,128)(2,1)S(1)}, u32[]{:S(2)}, u32[]{:S(2)}) collective-permute-start(bf16[96,2048]{1,0:T(8,128)(2,1)S(1)} %project.5), channel_id=1, source_target_pairs={{0,2},{1,5},{2,0},{3,7},{4,6},{5,1},{6,4},{7,3},{8,10},{9,13},{10,... | collective-permute-start | bytes 1179656 | tf_op jit(solution)/shard_map/ppermute | solution.py:426
  52.5 11.9 %collective-permute-start.12 = (bf16[96,2048]{1,0:T(8,128)(2,1)S(1)}, bf16[96,2048]{1,0:T(8,128)(2,1)S(1)}, u32[]{:S(2)}, u32[]{:S(2)}) collective-permute-start(bf16[96,2048]{1,0:T(8,128)(2,1)S(1)} %project.4), channel_id=1, source_target_pairs={{0,2},{1,5},{2,0},{3,7},{4,6},{5,1},{6,4},{7,3},{8,10},{9,13},{10,... | collective-permute-start | bytes 1179656 | tf_op jit(solution)/shard_map/ppermute | solution.py:428
  58.1 7.8 %collective-permute-start.14 = (bf16[96,2048]{1,0:T(8,128)(2,1)S(1)}, bf16[96,2048]{1,0:T(8,128)(2,1)S(1)}, u32[]{:S(2)}, u32[]{:S(2)}) collective-permute-start(bf16[96,2048]{1,0:T(8,128)(2,1)S(1)} %add_convert_fusion.1), channel_id=1, source_target_pairs={{0,4},{1,3},{2,6},{3,1},{4,0},{5,7},{6,2},{7,5},{8,12},{9,11},{10,... | collective-permute-start | bytes 1179656 | tf_op jit(solution)/shard_map/ppermute | solution.py:430
where the time goes:
time: 67 us; the launch traced here: 66.8 us
  waiting for transfers between devices  26 us (39%)
  Pallas kernels  20.4 us (30%)
  starting transfers between devices  19.3 us (29%)
  other arithmetic  0.94 us (1%)
    pallas_call x2, Pallas kernels, attend(): pl.pallas_call(functools.partial(attend_body, 256, len(blocks), state is...  4.99 us
    ppermute x1, waiting for transfers between devices, shards(): lax.ppermute(low[0], 'sp', forward)  4.86 us
    ppermute x1, waiting for transfers between devices, shards(): got = lax.ppermute(direct, 'tp', first_hop)  4.73 us
    ppermute x1, waiting for transfers between devices, shift(): low_b = lax.ppermute(low[1], 'sp', forward)  3.43 us
    ppermute x1, waiting for transfers between devices, shards(): got_on = lax.ppermute(pass_on, 'tp', first_hop)  3.43 us
    ppermute x1, starting transfers between devices, shift(): low_a = lax.ppermute(low[0], 'sp', forward)  3.11 us
    pallas_call x3, Pallas kernels, project(): pl.pallas_call(functools.partial(project_body, slots), out_shape=tuple((s...  3.05 us
    pallas_call x1, Pallas kernels, shards(): pl.pallas_call(second_keys_body, out_shape=rows_out + tuple((sds(w.shape,...  3.01 us
  transfers between devices with their start and end apart: 15, of which 9 were waited for; matrix products, arithmetic and copies ran while one was open for 0% of the time, Pallas kernels for 21%

commit v1 on v0

--- a/solution.py
+++ b/solution.py
@@ -192,10 +192,10 @@
     return new, add
 
 
-def attend_body(tile, blocks, first, *refs):
+def attend_body(tile, parts, first, *refs):
     q = refs[0]
-    kvs = refs[1 : 1 + 2 * blocks]
-    rest = refs[1 + 2 * blocks :]
+    kvs = refs[1 : 1 + sum(parts)]
+    rest = refs[1 + sum(parts) :]
     if first:
         w, lw, m_out, acc_out, w_v, lw_v, sems = rest
         copies = start_copies([(w, w_v), (lw, lw_v)], sems)
@@ -204,8 +204,10 @@
     for start in range(0, q.shape[0], tile):
         rows = pl.ds(start, tile)
         m, acc = (None, None) if first else (rest[0][rows, :], rest[1][rows, :])
-        for i in range(blocks):
-            m, acc = softmax_step(q[rows, :], kvs[2 * i : 2 * i + 2], m, acc)
+        used = 0
+        for count in parts:
+            m, acc = softmax_step(q[rows, :], kvs[used : used + count], m, acc)
+            used += count
         m_out[rows, :] = m
         acc_out[rows, :] = acc
     if first:
@@ -213,7 +215,7 @@
             copy.wait()
 
 
-def finish_body(flips, row_count, q, kva, kvb, m_in, acc_in, keep, send):
+def finish_body(flips, row_count, q, kv, m_in, acc_in, keep, send):
     _, core, pieces = place()
     piece = keep.shape[0] // len(flips)
     for i, flip in enumerate(flips):
@@ -221,7 +223,7 @@
         for h in range(q.shape[0] // row_count):
             start = h * row_count + (pieces[3] ^ flip) * 2 * piece
             rows = pl.ds(pl.multiple_of(start, 16), 2 * piece)
-            _, acc = softmax_step(q[rows, :], (kva, kvb), m_in[rows, :], acc_in[rows, :])
+            _, acc = softmax_step(q[rows, :], (kv,), m_in[rows, :], acc_in[rows, :])
             o = acc[:, :HEAD] / acc[:, HEAD:]
             lanes = slice(h * HEAD, (h + 1) * HEAD)
             keep[out_rows, lanes] = jnp.where(core == 0, o[:piece], o[piece:]).astype(bf16)
@@ -231,7 +233,7 @@
 def project_body(slots, keep, other, lkeep, lother, w, lw, w_other, lw_other, *outs):
     piece = outs[0].shape[-2]
     _, core, pieces = place()
-    held = (0, 1 + core, 2 - core, 3)
+    held = (0, core, 1 - core, 2)
     weights = jnp.concatenate([w[...], w_other[...], lw[...], lw_other[...]], axis=0)
     for slot, out in zip(slots, outs):
         rows = pl.ds(pl.multiple_of(held[slot] * piece, 16), piece)
@@ -270,7 +272,7 @@
     keys = sum(part.shape[0] for block in blocks for part in block)
     out_shape = (sds((rows, HEAD), f32), sds((rows, 2 * HEAD), f32)) + tuple(sds(a.shape, a.dtype) for a in bring)
     return pl.pallas_call(
-        functools.partial(attend_body, 256, len(blocks), state is None),
+        functools.partial(attend_body, 256, tuple(len(block) for block in blocks), state is None),
         out_shape=out_shape,
         in_specs=vmem(len(operands)) + hbm(len(bring)),
         out_specs=tuple(vmem(len(out_shape))),
@@ -280,19 +282,18 @@
     )(*operands, *in_hbm(*bring))
 
 
-def finish(q, block, state, flips, row_count, piece):
+def finish(q, kv, state, flips, row_count, piece):
     rows = q.shape[0]
-    keys = 2 * block[0].shape[0]
+    keys = kv.shape[0]
     done = 2 * piece * len(flips) * rows // row_count
     return pl.pallas_call(
         functools.partial(finish_body, flips, row_count),
         out_shape=(sds((piece * len(flips), rows // row_count * HEAD), bf16),) * 2,
-        in_specs=vmem(5),
+        in_specs=vmem(4),
         out_specs=tuple(vmem(2)),
         compiler_params=params(16),
         cost_estimate=cost(done * keys * HEAD * 8, done * keys),
-        name="finish",
-    )(q, *block, *state)
+    )(q, kv, *state)
 
 
 def project(slots, operands, piece, dtype):
@@ -305,7 +306,6 @@
         out_specs=tuple(vmem(len(slots))),
         compiler_params=params(8),
         cost_estimate=cost(2 * piece * width * depth * len(slots), 0, 4 * MIB),
-        name="project",
     )(*operands)
 
 
@@ -368,9 +368,9 @@
 
     def shift(low, high):
         low_a = lax.ppermute(low[0], "sp", forward)
+        high_b = lax.ppermute(high[1], "sp", backward)
+        low_b = lax.ppermute(low[1], "sp", forward)
         high_a = lax.ppermute(high[0], "sp", backward)
-        low_b = lax.ppermute(low[1], "sp", forward)
-        high_b = lax.ppermute(high[1], "sp", backward)
         return (low_a, low_b), (high_a, high_b)
 
     low, high = shift((kva, kvb), (kva, kvb))
@@ -396,12 +396,12 @@
     second_hop = [(i, i ^ (4 - 2 * (i % 2))) for i in range(n_tp)]
     low_edge = lax.ppermute(last_edge, "sp", forward[:-1])
     high_edge = lax.ppermute(first_edge, "sp", backward[:-1])
-    *state, w_own, lw_own = attend(q, [(kva, kvb), (low[0], high[0])], None, (grid_out_weight, local_out_weight))
+    *state, w_own, lw_own = attend(q, [(kva, kvb), (low[0], high[1])], None, (grid_out_weight, local_out_weight))
     w_other = lax.ppermute(w_own, "tp", flip)
     lw_other = lax.ppermute(lw_own, "tp", flip)
     for _ in range(1, (n_sp - 1) // 2):
         next_low, next_high = shift(low, high)
-        state = attend(q, [(low[1], high[1]), (next_low[0], next_high[0])], state)
+        state = attend(q, [(low[1], high[0]), (next_low[0], next_high[1])], state)
         low, high = next_low, next_high
     far = lax.ppermute(low[0], "sp", forward), lax.ppermute(high[1], "sp", backward)
 
@@ -416,19 +416,24 @@
         name="banded",
     )(sink_logit.reshape(1, heads), lq, lkv, low_edge, high_edge)
     lother = lax.ppermute(lsend, "tp", flip)
-    state = attend(q, [(low[1], high[1])], state)
+    state = attend(q, [(low[1], high[0])], state)
 
     piece = row_count // n_tp
-    keep, send = finish(q, far, state, (3, 1, 2, 0), row_count, piece)
+    state = attend(q, [(far[0],)], state)
+    keep, send = finish(q, far[1], state, (3,), row_count, piece)
     other = lax.ppermute(send, "tp", flip)
-    operands = (keep, other, lkeep, lother, w_own, lw_own, w_other, lw_other)
-    (pass_on,) = project((0,), operands, piece, bf16)
+    keep_rest, send_rest = finish(q, far[1], state, (1, 2, 0), row_count, piece)
+    other_rest = lax.ppermute(send_rest, "tp", flip)
+
+    fixed = (lkeep, lother, w_own, lw_own, w_other, lw_other)
+    (pass_on,) = project((0,), (keep, other) + fixed, piece, bf16)
     got_on = lax.ppermute(pass_on, "tp", first_hop)
-    (direct,) = project((1,), operands, piece, bf16)
+    next_part, own_part = project((2, 3), (keep_rest, other_rest) + fixed, piece, f32)
+    (direct,) = project((1,), (keep_rest, other_rest) + fixed, piece, bf16)
     got = lax.ppermute(direct, "tp", first_hop)
-    next_part, own_part = project((2, 3), operands, piece, f32)
     got_next = lax.ppermute((next_part + got_on.astype(f32)).astype(bf16), "tp", second_hop)
-    return (own_part + got.astype(f32) + got_next.astype(f32)).astype(bf16)
+    summed = lax.optimization_barrier(own_part + got.astype(f32))
+    return (summed + got_next.astype(f32)).astype(bf16)
 
 
 def solution(mesh):

time: 67 us -> 69.8 us (1.042)
  Pallas kernels: 20.4 us -> 22 us
  starting transfers between devices: 19.3 us -> 20.4 us
    ppermute x1, waiting for transfers between devices: 0.01 us -> 5.33 us  [shards(): high_edge = lax.ppermute(first_edge, 'sp', backward[:-1])]
    ppermute x1, waiting for transfers between devices: 0.01 us -> 3.99 us  [shift(): low_a = lax.ppermute(low[0], 'sp', forward)]
    ppermute x1, waiting for transfers between devices: 4.86 us -> 1.38 us  [shards(): lax.ppermute(low[0], 'sp', forward)]
    ppermute x1, waiting for transfers between devices: 3.43 us -> 0.01 us  [shift(): low_b = lax.ppermute(low[1], 'sp', forward)]
    ppermute x1, waiting for transfers between devices: 3.43 us -> 0.13 us  [shards(): got_on = lax.ppermute(pass_on, 'tp', first_hop)]
    ppermute x1, starting transfers between devices: 3.11 us -> 0.01 us  [shift(): low_a = lax.ppermute(low[0], 'sp', forward)]
    ppermute x1, starting transfers between devices: 2.31 us -> 5.12 us  [shift(): high_b = lax.ppermute(high[1], 'sp', backward)]
    ppermute x1, waiting for transfers between devices: 2.72 us -> 0.01 us  [shift(): high_a = lax.ppermute(high[0], 'sp', backward)]
  transfers between devices with their start and end apart: 15 -> 16, of which waited for: 9 -> 10; matrix products, arithmetic and copies ran while one was open for 0% -> 0% of each run, Pallas kernels for 21% -> 18%
where the time goes in v1:
time: 69.8 us; the launch traced here: 69.5 us
  waiting for transfers between devices  25.9 us (37%)
  Pallas kernels  22 us (32%)
  starting transfers between devices  20.4 us (29%)
  other arithmetic  0.97 us (1%)
    pallas_call x3, Pallas kernels, attend(): pl.pallas_call(functools.partial(attend_body, 256, tuple((len(block) for...  6.51 us
    ppermute x1, waiting for transfers between devices, shards(): got = lax.ppermute(direct, 'tp', first_hop)  5.67 us
    ppermute x1, waiting for transfers between devices, shards(): high_edge = lax.ppermute(first_edge, 'sp', backward[:-1])  5.33 us
    ppermute x1, starting transfers between devices, shift(): high_b = lax.ppermute(high[1], 'sp', backward)  5.12 us
    ppermute x1, waiting for transfers between devices, shift(): low_a = lax.ppermute(low[0], 'sp', forward)  3.99 us
    ppermute x1, waiting for transfers between devices, shards(): low_edge = lax.ppermute(last_edge, 'sp', forward[:-1])  3.14 us
    pallas_call x3, Pallas kernels, project(): pl.pallas_call(functools.partial(project_body, slots), out_shape=tuple((s...  3.05 us
    pallas_call x1, Pallas kernels, shards(): pl.pallas_call(second_keys_body, out_shape=rows_out + tuple((sds(w.shape,...  3.02 us
  transfers between devices with their start and end apart: 16, of which 10 were waited for; matrix products, arithmetic and copies ran while one was open for 0% of the time, Pallas kernels for 18%

profile of v1, /device:TPU:0, one launch (start us, length us, event | category | flops | bytes accessed | tf_op | source)
XLA Modules:
  0.0 69.5 jit_solution(9682394985120988238)
XLA Ops:
  0.0 2.7 %keys_a.1 = (bf16[384,2048]{1,0:T(8,128)(2,1)S(1)}, bf16[384,256]{1,0:T(8,128)(2,1)S(1)}, bf16[384,2048]{1,0:T(8,128)(2,1)S(1)}, f32[1,2048]{1,0:T(1,128)S(1)}, ...) custom-call(bf16[768,2048]{1,0:T(8,128)(2,1)} %tok.1, ...), custom_call_target="tpu_custom_call" | custom-call | flops 120795952 | bytes 4194304 | tf_op jit(solution)/shard_map/keys_a/pallas_call | solution.py:344
  2.7 3.0 %keys_b.1 = (bf16[384,2048]{1,0:T(8,128)(2,1)S(1)}, bf16[384,256]{1,0:T(8,128)(2,1)S(1)}, bf16[2048,256]{1,0:T(8,128)(2,1)S(1)}, bf16[2048,256]{1,0:T(8,128)(2,1...) custom-call(bf16[384,2048]{1,0:T(8,128)(2,1)S(1)} %get-tuple-element.43.tok, ...), custom_call_target="tpu_custom_call" | custom-call | flops 120795952 | bytes 4194304 | tf_op jit(solution)/shard_map/keys_b/pallas_call | solution.py:354
  5.7 5.1 %collective-permute-start = (bf16[384,256]{1,0:T(8,128)(2,1)S(1)}, bf16[384,256]{1,0:T(8,128)(2,1)S(1)}, u32[]{:S(2)}, u32[]{:S(2)}) collective-permute-start(bf16[384,256]{1,0:T(8,128)(2,1)S(1)} %get-tuple-element.57.refs_2_), channel_id=1, source_target_pairs={{8,0},{16,8},{24,16},{0,24},{9,1},{17,9},{25,17},{1,25},{10,2},{18... | collective-permute-start | bytes 589832 | tf_op jit(solution)/shard_map/ppermute | solution.py:371
  10.8 0.0 collective-permute-start.2
  10.8 2.7 %queries.1 = (bf16[1536,128]{1,0:T(8,128)(2,1)S(1)}, bf16[768,256]{1,0:T(8,128)(2,1)S(1)}, bf16[768,256]{1,0:T(8,128)(2,1)S(1)}, bf16[128,256]{1,0:T(8,128)(2,1)S(1)}, bf16[128,256]{1,0:T(8,128)(2,1)S(1)}) custom-call(bf16[384,2048]{1,0:T(8,128)(2,1)S(1)} %get-tuple-element.42.normed_a, bf16[384,2048]{1,0:T(8,128)(2,1)S(1)} %get-tuple-element.50.normed_b, ...), custom_call_target="tpu_custom_call" | custom-call | flops 724775744 | bytes 6291456 | tf_op jit(solution)/shard_map/queries/pallas_call | solution.py:378
  13.6 2.5 %collective-permute-done.refs_4_ = bf16[384,256]{1,0:T(8,128)(2,1)S(1)} collective-permute-done((bf16[384,256]{1,0:T(8,128)(2,1)S(1)}, bf16[384,256]{1,0:T(8,128)(2,1)S(1)}, u32[]{:S(2)}, u32[]{:S(2)}) %collective-permute-start) | collective-permute-done | bytes 196640 | tf_op jit(solution)/shard_map/ppermute | solution.py:371
  16.1 4.0 %collective-permute-done.2.refs_3_ = bf16[384,256]{1,0:T(8,128)(2,1)S(1)} collective-permute-done((bf16[384,256]{1,0:T(8,128)(2,1)S(1)}, bf16[384,256]{1,0:T(8,128)(2,1)S(1)}, u32[]{:S(2)}, u32[]{:S(2)}) %collective-permute-start.2) | collective-permute-done | bytes 196640 | tf_op jit(solution)/shard_map/ppermute | solution.py:370
  20.1 3.1 %shard_map.145 = (f32[1536,128]{1,0:T(8,128)S(1)}, f32[1536,256]{1,0:T(8,128)S(1)}, bf16[256,2048]{1,0:T(8,128)(2,1)S(1)}, bf16[256,2048]{1,0:T(8,128)(2,1)S(1)}) custom-call(bf16[1536,128]{1,0:T(8,128)(2,1)S(1)} %get-tuple-element.56.refs_0_.q, bf16[384,256]{1,0:T(8,128)(2,1)S(1)} %get-tuple-element.58.refs_1_, ...), custom_call_target="tpu_custom_call" | custom-call | flops 724775744 | tf_op jit(solution)/shard_map/pallas_call | solution.py:274
  23.2 0.1 collective-permute-start.10
  23.3 0.5 collective-permute-start.11
  23.8 1.6 %collective-permute-start.4 = (bf16[384,256]{1,0:T(8,128)(2,1)S(1)}, bf16[384,256]{1,0:T(8,128)(2,1)S(1)}, u32[]{:S(2)}, u32[]{:S(2)}) collective-permute-start(bf16[384,256]{1,0:T(8,128)(2,1)S(1)} %get-tuple-element.57.refs_2_), channel_id=1, source_target_pairs={{0,8},{8,16},{16,24},{24,0},{1,9},{9,17},{17,25},{25,1},{2,10},{10... | collective-permute-start | bytes 589832 | tf_op jit(solution)/shard_map/ppermute | solution.py:372
  25.4 1.9 %collective-permute-start.7 = (bf16[128,256]{1,0:T(8,128)(2,1)S(1)}, bf16[128,256]{1,0:T(8,128)(2,1)S(1)}, u32[]{:S(2)}, u32[]{:S(2)}) collective-permute-start(bf16[128,256]{1,0:T(8,128)(2,1)S(1)} %get-tuple-element.69), channel_id=1, source_target_pairs={{0,8},{8,16},{16,24},{1,9},{9,17},{17,25},{2,10},{10,18},{18,26},{... | collective-permute-start | bytes 196616 | tf_op jit(solution)/shard_map/ppermute | solution.py:397
  27.3 1.6 %collective-permute-start.5 = (bf16[384,256]{1,0:T(8,128)(2,1)S(1)}, bf16[384,256]{1,0:T(8,128)(2,1)S(1)}, u32[]{:S(2)}, u32[]{:S(2)}) collective-permute-start(bf16[384,256]{1,0:T(8,128)(2,1)S(1)} %get-tuple-element.58.refs_1_), channel_id=1, source_target_pairs={{8,0},{16,8},{24,16},{0,24},{9,1},{17,9},{25,17},{1,25},{10,2},{18... | collective-permute-start | bytes 589832 | tf_op jit(solution)/shard_map/ppermute | solution.py:373
  28.9 3.1 %collective-permute-done.7.low = bf16[128,256]{1,0:T(8,128)(2,1)S(1)} collective-permute-done((bf16[128,256]{1,0:T(8,128)(2,1)S(1)}, bf16[128,256]{1,0:T(8,128)(2,1)S(1)}, u32[]{:S(2)}, u32[]{:S(2)}) %collective-permute-start.7) | collective-permute-done | bytes 65568 | tf_op jit(solution)/shard_map/ppermute | solution.py:397
  32.1 1.3 %collective-permute-start.8 = (bf16[128,256]{1,0:T(8,128)(2,1)S(1)}, bf16[128,256]{1,0:T(8,128)(2,1)S(1)}, u32[]{:S(2)}, u32[]{:S(2)}) collective-permute-start(bf16[128,256]{1,0:T(8,128)(2,1)S(1)} %get-tuple-element.70), channel_id=1, source_target_pairs={{8,0},{16,8},{24,16},{9,1},{17,9},{25,17},{10,2},{18,10},{26,18},{... | collective-permute-start | bytes 196616 | tf_op jit(solution)/shard_map/ppermute | solution.py:398
  33.4 5.3 %collective-permute-done.8.high = bf16[128,256]{1,0:T(8,128)(2,1)S(1)} collective-permute-done((bf16[128,256]{1,0:T(8,128)(2,1)S(1)}, bf16[128,256]{1,0:T(8,128)(2,1)S(1)}, u32[]{:S(2)}, u32[]{:S(2)}) %collective-permute-start.8) | collective-permute-done | bytes 65568 | tf_op jit(solution)/shard_map/ppermute | solution.py:398
  38.7 2.0 %collective-permute-start.3 = (bf16[384,256]{1,0:T(8,128)(2,1)S(1)}, bf16[384,256]{1,0:T(8,128)(2,1)S(1)}, u32[]{:S(2)}, u32[]{:S(2)}) collective-permute-start(bf16[384,256]{1,0:T(8,128)(2,1)S(1)} %collective-permute-done.2.refs_3_), channel_id=1, source_target_pairs={{0,8},{8,16},{16,24},{24,0},{1,9},{9,17},{17,25},{25,1},{2,10},{10... | collective-permute-start | bytes 589832 | tf_op jit(solution)/shard_map/ppermute | solution.py:406
  40.7 0.0 collective-permute-done.4.refs_1_
  40.7 1.8 %collective-permute-start.1 = (bf16[384,256]{1,0:T(8,128)(2,1)S(1)}, bf16[384,256]{1,0:T(8,128)(2,1)S(1)}, u32[]{:S(2)}, u32[]{:S(2)}) collective-permute-start(bf16[384,256]{1,0:T(8,128)(2,1)S(1)} %collective-permute-done.refs_4_), channel_id=1, source_target_pairs={{8,0},{16,8},{24,16},{0,24},{9,1},{17,9},{25,17},{1,25},{10,2},{18... | collective-permute-start | bytes 589832 | tf_op jit(solution)/shard_map/ppermute | solution.py:406
  42.5 0.0 copy-done
  42.5 2.1 %banded.1 = (bf16[384,256]{1,0:T(8,128)(2,1)S(1)}, bf16[384,256]{1,0:T(8,128)(2,1)S(1)}) custom-call(f32[1,2]{1,0:T(1,128)S(1)} %bitcast.4, bf16[768,256]{1,0:T(8,128)(2,1)S(1)} %get-tuple-element.67.lq, bf16[768,256]{1,0:T(8,128)(2,1)S(1)} %get-tuple-element.68.lkv, bf16[128,256]{1,0:T(8,128)(2,1)S(1)} %collective-permute-done.7.low, ...), custom_call_target="tpu_custom_call" | custom-call | flops 181193936 | tf_op jit(solution)/shard_map/banded/pallas_call | solution.py:408
  44.6 0.0 collective-permute-done.5.refs_2_
  44.6 0.1 collective-permute-start.9
  44.7 1.9 %shard_map.146 = (f32[1536,128]{1,0:T(8,128)S(1)}, f32[1536,256]{1,0:T(8,128)S(1)}) custom-call(bf16[1536,128]{1,0:T(8,128)(2,1)S(1)} %get-tuple-element.56.refs_0_.q, bf16[384,256]{1,0:T(8,128)(2,1)S(1)} %collective-permute-done.4.refs_1_, bf16[384,256]{1,0:T(8,128)(2,1)S(1)} %collective-permute-done.5.refs_2_, f32[1536,128]{1,0:T(8,128)S(1)} %get-tuple-element.59.refs_3_, ...), custom_call_target="tpu_custom_call" | custom-call | flops 362387872 | tf_op jit(solution)/shard_map/pallas_call | solution.py:274
  46.6 1.4 %collective-permute-done.3.refs_1_ = bf16[384,256]{1,0:T(8,128)(2,1)S(1)} collective-permute-done((bf16[384,256]{1,0:T(8,128)(2,1)S(1)}, bf16[384,256]{1,0:T(8,128)(2,1)S(1)}, u32[]{:S(2)}, u32[]{:S(2)}) %collective-permute-start.3) | collective-permute-done | bytes 196640 | tf_op jit(solution)/shard_map/ppermute | solution.py:406
  48.0 1.6 %shard_map.147 = (f32[1536,128]{1,0:T(8,128)S(1)}, f32[1536,256]{1,0:T(8,128)S(1)}) custom-call(bf16[1536,128]{1,0:T(8,128)(2,1)S(1)} %get-tuple-element.56.refs_0_.q, bf16[384,256]{1,0:T(8,128)(2,1)S(1)} %collective-permute-done.3.refs_1_, f32[1536,128]{1,0:T(8,128)S(1)} %get-tuple-element.61.refs_2_, f32[1536,256]{1,0:T(8,128)S(1)} %get-tuple-element.62.refs_3_), custom_call_target="tpu_custom_call" | custom-call | flops 181193936 | tf_op jit(solution)/shard_map/pallas_call | solution.py:274
  49.5 0.0 collective-permute-done.1.kv
  49.6 0.6 shard_map.151
  50.1 0.1 collective-permute-start.13
  50.2 0.0 collective-permute-done.9.lother
  50.2 1.2 %collective-permute-done.13.other = bf16[96,256]{1,0:T(8,128)(2,1)S(1)} collective-permute-done((bf16[96,256]{1,0:T(8,128)(2,1)S(1)}, bf16[96,256]{1,0:T(8,128)(2,1)S(1)}, u32[]{:S(2)}, u32[]{:S(2)}) %collective-permute-start.13) | collective-permute-done | bytes 49184 | tf_op jit(solution)/shard_map/ppermute | solution.py:424
  51.4 0.0 collective-permute-done.10.w_other
  51.4 0.0 collective-permute-done.11.lw_other
  51.4 0.8 %shard_map.152 = bf16[96,2048]{1,0:T(8,128)(2,1)S(1)} custom-call(bf16[96,256]{1,0:T(8,128)(2,1)S(1)} %get-tuple-element.77.keep, bf16[96,256]{1,0:T(8,128)(2,1)S(1)} %collective-permute-done.13.other, bf16[384,256]{1,0:T(8,128)(2,1)S(1)} %get-tuple-element.71.lkeep, bf16[384,256]{1,0:T(8,128)(2,1)S(1)} %collective-permute-done.9.lother, ...), custom_call_target="tpu_custom_call" | custom-call | flops 120795952 | bytes 4194304 | tf_op jit(solution)/shard_map/pallas_call | solution.py:302
  52.2 1.6 %collective-permute-start.14 = (bf16[96,2048]{1,0:T(8,128)(2,1)S(1)}, bf16[96,2048]{1,0:T(8,128)(2,1)S(1)}, u32[]{:S(2)}, u32[]{:S(2)}) collective-permute-start(bf16[96,2048]{1,0:T(8,128)(2,1)S(1)} %shard_map.152), channel_id=1, source_target_pairs={{0,2},{1,5},{2,0},{3,7},{4,6},{5,1},{6,4},{7,3},{8,10},{9,13},{10,... | collective-permute-start | bytes 1179656 | tf_op jit(solution)/shard_map/ppermute | solution.py:430
  53.8 1.4 %shard_map.148 = (bf16[288,256]{1,0:T(8,128)(2,1)S(1)}, bf16[288,256]{1,0:T(8,128)(2,1)S(1)}) custom-call(bf16[1536,128]{1,0:T(8,128)(2,1)S(1)} %get-tuple-element.56.refs_0_.q, bf16[384,256]{1,0:T(8,128)(2,1)S(1)} %collective-permute-done.1.kv, f32[1536,128]{1,0:T(8,128)S(1)} %get-tuple-element.63.m_in, f32[1536,256]{1,0:T(8,128)S(1)} %get-tuple-element.64.acc_in), custom_call_target="tpu_custom_call" | custom-call | flops 135895456 | tf_op jit(solution)/shard_map/pallas_call | solution.py:289
  55.2 0.1 collective-permute-start.6
  55.2 1.4 %collective-permute-done.6.other = bf16[288,256]{1,0:T(8,128)(2,1)S(1)} collective-permute-done((bf16[288,256]{1,0:T(8,128)(2,1)S(1)}, bf16[288,256]{1,0:T(8,128)(2,1)S(1)}, u32[]{:S(2)}, u32[]{:S(2)}) %collective-permute-start.6) | collective-permute-done | bytes 147488 | tf_op jit(solution)/shard_map/ppermute | solution.py:426
  56.6 0.8 %shard_map.150 = bf16[96,2048]{1,0:T(8,128)(2,1)S(1)} custom-call(bf16[288,256]{1,0:T(8,128)(2,1)S(1)} %get-tuple-element.65.keep, bf16[288,256]{1,0:T(8,128)(2,1)S(1)} %collective-permute-done.6.other, bf16[384,256]{1,0:T(8,128)(2,1)S(1)} %get-tuple-element.71.lkeep, bf16[384,256]{1,0:T(8,128)(2,1)S(1)} %collective-permute-done.9.lother, ...), custom_call_target="tpu_custom_call" | custom-call | flops 120795952 | bytes 4194304 | tf_op jit(solution)/shard_map/pallas_call | solution.py:302
  57.4 1.1 %collective-permute-start.12 = (bf16[96,2048]{1,0:T(8,128)(2,1)S(1)}, bf16[96,2048]{1,0:T(8,128)(2,1)S(1)}, u32[]{:S(2)}, u32[]{:S(2)}) collective-permute-start(bf16[96,2048]{1,0:T(8,128)(2,1)S(1)} %shard_map.150), channel_id=1, source_target_pairs={{0,2},{1,5},{2,0},{3,7},{4,6},{5,1},{6,4},{7,3},{8,10},{9,13},{10,... | collective-permute-start | bytes 1179656 | tf_op jit(solution)/shard_map/ppermute | solution.py:433
  58.5 1.5 %shard_map.149 = (f32[96,2048]{1,0:T(8,128)S(1)}, f32[96,2048]{1,0:T(8,128)S(1)}) custom-call(bf16[288,256]{1,0:T(8,128)(2,1)S(1)} %get-tuple-element.65.keep, bf16[288,256]{1,0:T(8,128)(2,1)S(1)} %collective-permute-done.6.other, bf16[384,256]{1,0:T(8,128)(2,1)S(1)} %get-tuple-element.71.lkeep, bf16[384,256]{1,0:T(8,128)(2,1)S(1)} %collective-permute-done.9.lother, ...), custom_call_target="tpu_custom_call" | custom-call | flops 241591904 | bytes 4194304 | tf_op jit(solution)/shard_map/pallas_call | solution.py:302
  60.0 0.1 collective-permute-done.14
  60.1 0.1 add_convert_fusion.1
  60.2 1.6 %collective-permute-start.15 = (bf16[96,2048]{1,0:T(8,128)(2,1)S(1)}, bf16[96,2048]{1,0:T(8,128)(2,1)S(1)}, u32[]{:S(2)}, u32[]{:S(2)}) collective-permute-start(bf16[96,2048]{1,0:T(8,128)(2,1)S(1)} %add_convert_fusion.1), channel_id=1, source_target_pairs={{0,4},{1,3},{2,6},{3,1},{4,0},{5,7},{6,2},{7,5},{8,12},{9,11},{10,... | collective-permute-start | bytes 1179656 | tf_op jit(solution)/shard_map/ppermute | solution.py:434
  61.8 5.7 %collective-permute-done.12 = bf16[96,2048]{1,0:T(8,128)(2,1)S(1)} collective-permute-done((bf16[96,2048]{1,0:T(8,128)(2,1)S(1)}, bf16[96,2048]{1,0:T(8,128)(2,1)S(1)}, u32[]{:S(2)}, u32[]{:S(2)}) %collective-permute-start.12) | collective-permute-done | bytes 393248 | tf_op jit(solution)/shard_map/ppermute | solution.py:433
  67.4 0.1 convert_add_fusion
  67.5 1.1 %collective-permute-done.15 = bf16[96,2048]{1,0:T(8,128)(2,1)S(1)} collective-permute-done((bf16[96,2048]{1,0:T(8,128)(2,1)S(1)}, bf16[96,2048]{1,0:T(8,128)(2,1)S(1)}, u32[]{:S(2)}, u32[]{:S(2)}) %collective-permute-start.15) | collective-permute-done | bytes 393248 | tf_op jit(solution)/shard_map/ppermute | solution.py:434
  68.6 0.8 %add_convert_fusion = bf16[96,2048]{1,0:T(8,128)(2,1)} fusion(f32[96,2048]{1,0:T(8,128)S(1)} %convert_add_fusion, bf16[96,2048]{1,0:T(8,128)(2,1)S(1)} %collective-permute-done.15), kind=kLoop, calls=%fused_computation | loop fusion | flops 589824 | bytes 1572864 | tf_op jit(solution)/shard_map/convert_element_type | solution.py:436
  (1 shorter events, 0.0 us)
Async XLA Ops:
  5.7 10.4 %collective-permute-start = (bf16[384,256]{1,0:T(8,128)(2,1)S(1)}, bf16[384,256]{1,0:T(8,128)(2,1)S(1)}, u32[]{:S(2)}, u32[]{:S(2)}) collective-permute-start(bf16[384,256]{1,0:T(8,128)(2,1)S(1)} %get-tuple-element.57.refs_2_), channel_id=1, source_target_pairs={{8,0},{16,8},{24,16},{0,24},{9,1},{17,9},{25,17},{1,25},{10,2},{18... | collective-permute-start | bytes 589832 | tf_op jit(solution)/shard_map/ppermute | solution.py:371
  10.8 9.3 %collective-permute-start.2 = (bf16[384,256]{1,0:T(8,128)(2,1)S(1)}, bf16[384,256]{1,0:T(8,128)(2,1)S(1)}, u32[]{:S(2)}, u32[]{:S(2)}) collective-permute-start(bf16[384,256]{1,0:T(8,128)(2,1)S(1)} %get-tuple-element.58.refs_1_), channel_id=1, source_target_pairs={{0,8},{8,16},{16,24},{24,0},{1,9},{9,17},{17,25},{25,1},{2,10},{10... | collective-permute-start | bytes 589832 | tf_op jit(solution)/shard_map/ppermute | solution.py:370
  20.1 22.4 %copy-start = (f32[2]{0:T(128)S(1)}, f32[2]{0:T(128)}, u32[]{:S(2)}) copy-start(f32[2]{0:T(128)} %param.25) | copy-start | bytes 28
  23.2 28.2 %collective-permute-start.10 = (bf16[256,2048]{1,0:T(8,128)(2,1)S(1)}, bf16[256,2048]{1,0:T(8,128)(2,1)S(1)}, u32[]{:S(2)}, u32[]{:S(2)}) collective-permute-start(bf16[256,2048]{1,0:T(8,128)(2,1)S(1)} %get-tuple-element.73.w), channel_id=1, source_target_pairs={{0,1},{1,0},{2,3},{3,2},{4,5},{5,4},{6,7},{7,6},{8,9},{9,8},{10,11... | collective-permute-start | bytes 3145736 | tf_op jit(solution)/shard_map/ppermute | solution.py:400
  23.3 28.2 %collective-permute-start.11 = (bf16[256,2048]{1,0:T(8,128)(2,1)S(1)}, bf16[256,2048]{1,0:T(8,128)(2,1)S(1)}, u32[]{:S(2)}, u32[]{:S(2)}) collective-permute-start(bf16[256,2048]{1,0:T(8,128)(2,1)S(1)} %get-tuple-element.74.lw), channel_id=1, source_target_pairs={{0,1},{1,0},{2,3},{3,2},{4,5},{5,4},{6,7},{7,6},{8,9},{9,8},{10,11... | collective-permute-start | bytes 3145736 | tf_op jit(solution)/shard_map/ppermute | solution.py:401
  23.8 16.9 %collective-permute-start.4 = (bf16[384,256]{1,0:T(8,128)(2,1)S(1)}, bf16[384,256]{1,0:T(8,128)(2,1)S(1)}, u32[]{:S(2)}, u32[]{:S(2)}) collective-permute-start(bf16[384,256]{1,0:T(8,128)(2,1)S(1)} %get-tuple-element.57.refs_2_), channel_id=1, source_target_pairs={{0,8},{8,16},{16,24},{24,0},{1,9},{9,17},{17,25},{25,1},{2,10},{10... | collective-permute-start | bytes 589832 | tf_op jit(solution)/shard_map/ppermute | solution.py:372
  25.4 6.7 %collective-permute-start.7 = (bf16[128,256]{1,0:T(8,128)(2,1)S(1)}, bf16[128,256]{1,0:T(8,128)(2,1)S(1)}, u32[]{:S(2)}, u32[]{:S(2)}) collective-permute-start(bf16[128,256]{1,0:T(8,128)(2,1)S(1)} %get-tuple-element.69), channel_id=1, source_target_pairs={{0,8},{8,16},{16,24},{1,9},{9,17},{17,25},{2,10},{10,18},{18,26},{... | collective-permute-start | bytes 196616 | tf_op jit(solution)/shard_map/ppermute | solution.py:397
  27.3 17.3 %collective-permute-start.5 = (bf16[384,256]{1,0:T(8,128)(2,1)S(1)}, bf16[384,256]{1,0:T(8,128)(2,1)S(1)}, u32[]{:S(2)}, u32[]{:S(2)}) collective-permute-start(bf16[384,256]{1,0:T(8,128)(2,1)S(1)} %get-tuple-element.58.refs_1_), channel_id=1, source_target_pairs={{8,0},{16,8},{24,16},{0,24},{9,1},{17,9},{25,17},{1,25},{10,2},{18... | collective-permute-start | bytes 589832 | tf_op jit(solution)/shard_map/ppermute | solution.py:373
  32.1 6.6 %collective-permute-start.8 = (bf16[128,256]{1,0:T(8,128)(2,1)S(1)}, bf16[128,256]{1,0:T(8,128)(2,1)S(1)}, u32[]{:S(2)}, u32[]{:S(2)}) collective-permute-start(bf16[128,256]{1,0:T(8,128)(2,1)S(1)} %get-tuple-element.70), channel_id=1, source_target_pairs={{8,0},{16,8},{24,16},{9,1},{17,9},{25,17},{10,2},{18,10},{26,18},{... | collective-permute-start | bytes 196616 | tf_op jit(solution)/shard_map/ppermute | solution.py:398
  38.7 9.2 %collective-permute-start.3 = (bf16[384,256]{1,0:T(8,128)(2,1)S(1)}, bf16[384,256]{1,0:T(8,128)(2,1)S(1)}, u32[]{:S(2)}, u32[]{:S(2)}) collective-permute-start(bf16[384,256]{1,0:T(8,128)(2,1)S(1)} %collective-permute-done.2.refs_3_), channel_id=1, source_target_pairs={{0,8},{8,16},{16,24},{24,0},{1,9},{9,17},{17,25},{25,1},{2,10},{10... | collective-permute-start | bytes 589832 | tf_op jit(solution)/shard_map/ppermute | solution.py:406
  40.7 8.8 %collective-permute-start.1 = (bf16[384,256]{1,0:T(8,128)(2,1)S(1)}, bf16[384,256]{1,0:T(8,128)(2,1)S(1)}, u32[]{:S(2)}, u32[]{:S(2)}) collective-permute-start(bf16[384,256]{1,0:T(8,128)(2,1)S(1)} %collective-permute-done.refs_4_), channel_id=1, source_target_pairs={{8,0},{16,8},{24,16},{0,24},{9,1},{17,9},{25,17},{1,25},{10,2},{18... | collective-permute-start | bytes 589832 | tf_op jit(solution)/shard_map/ppermute | solution.py:406
  44.6 5.6 %collective-permute-start.9 = (bf16[384,256]{1,0:T(8,128)(2,1)S(1)}, bf16[384,256]{1,0:T(8,128)(2,1)S(1)}, u32[]{:S(2)}, u32[]{:S(2)}) collective-permute-start(bf16[384,256]{1,0:T(8,128)(2,1)S(1)} %get-tuple-element.72), channel_id=1, source_target_pairs={{0,1},{1,0},{2,3},{3,2},{4,5},{5,4},{6,7},{7,6},{8,9},{9,8},{10,11... | collective-permute-start | bytes 589832 | tf_op jit(solution)/shard_map/ppermute | solution.py:418
  50.1 1.3 %collective-permute-start.13 = (bf16[96,256]{1,0:T(8,128)(2,1)S(1)}, bf16[96,256]{1,0:T(8,128)(2,1)S(1)}, u32[]{:S(2)}, u32[]{:S(2)}) collective-permute-start(bf16[96,256]{1,0:T(8,128)(2,1)S(1)} %get-tuple-element.78), channel_id=1, source_target_pairs={{0,1},{1,0},{2,3},{3,2},{4,5},{5,4},{6,7},{7,6},{8,9},{9,8},{10,11... | collective-permute-start | bytes 147464 | tf_op jit(solution)/shard_map/ppermute | solution.py:424
  52.2 7.8 %collective-permute-start.14 = (bf16[96,2048]{1,0:T(8,128)(2,1)S(1)}, bf16[96,2048]{1,0:T(8,128)(2,1)S(1)}, u32[]{:S(2)}, u32[]{:S(2)}) collective-permute-start(bf16[96,2048]{1,0:T(8,128)(2,1)S(1)} %shard_map.152), channel_id=1, source_target_pairs={{0,2},{1,5},{2,0},{3,7},{4,6},{5,1},{6,4},{7,3},{8,10},{9,13},{10,... | collective-permute-start | bytes 1179656 | tf_op jit(solution)/shard_map/ppermute | solution.py:430
  55.2 1.4 %collective-permute-start.6 = (bf16[288,256]{1,0:T(8,128)(2,1)S(1)}, bf16[288,256]{1,0:T(8,128)(2,1)S(1)}, u32[]{:S(2)}, u32[]{:S(2)}) collective-permute-start(bf16[288,256]{1,0:T(8,128)(2,1)S(1)} %get-tuple-element.66), channel_id=1, source_target_pairs={{0,1},{1,0},{2,3},{3,2},{4,5},{5,4},{6,7},{7,6},{8,9},{9,8},{10,11... | collective-permute-start | bytes 442376 | tf_op jit(solution)/shard_map/ppermute | solution.py:426
  57.4 10.0 %collective-permute-start.12 = (bf16[96,2048]{1,0:T(8,128)(2,1)S(1)}, bf16[96,2048]{1,0:T(8,128)(2,1)S(1)}, u32[]{:S(2)}, u32[]{:S(2)}) collective-permute-start(bf16[96,2048]{1,0:T(8,128)(2,1)S(1)} %shard_map.150), channel_id=1, source_target_pairs={{0,2},{1,5},{2,0},{3,7},{4,6},{5,1},{6,4},{7,3},{8,10},{9,13},{10,... | collective-permute-start | bytes 1179656 | tf_op jit(solution)/shard_map/ppermute | solution.py:433
  60.2 8.5 %collective-permute-start.15 = (bf16[96,2048]{1,0:T(8,128)(2,1)S(1)}, bf16[96,2048]{1,0:T(8,128)(2,1)S(1)}, u32[]{:S(2)}, u32[]{:S(2)}) collective-permute-start(bf16[96,2048]{1,0:T(8,128)(2,1)S(1)} %add_convert_fusion.1), channel_id=1, source_target_pairs={{0,4},{1,3},{2,6},{3,1},{4,0},{5,7},{6,2},{7,5},{8,12},{9,11},{10,... | collective-permute-start | bytes 1179656 | tf_op jit(solution)/shard_map/ppermute | solution.py:434

commit v2 on v1

--- a/solution.py
+++ b/solution.py
@@ -230,6 +230,17 @@
             send[out_rows, lanes] = jnp.where(core == 0, o[piece:], o[:piece]).astype(bf16)
 
 
+def early_body(keep, lkeep, lother, w, lw, lw_other, out):
+    piece = keep.shape[0]
+    lrows = pl.ds(pl.multiple_of(place()[2][0] * piece, 16), piece)
+    part = jnp.concatenate([keep[...], lkeep[lrows, :], lother[lrows, :]], axis=1)
+    out[...] = dot(part, jnp.concatenate([w[...], lw[...], lw_other[...]], axis=0))
+
+
+def pass_body(early, other, w_other, out):
+    out[...] = (early[...] + dot(other[...], w_other[...])).astype(out.dtype)
+
+
 def project_body(slots, keep, other, lkeep, lother, w, lw, w_other, lw_other, *outs):
     piece = outs[0].shape[-2]
     _, core, pieces = place()
@@ -368,9 +379,9 @@
 
     def shift(low, high):
         low_a = lax.ppermute(low[0], "sp", forward)
+        high_a = lax.ppermute(high[0], "sp", backward)
+        low_b = lax.ppermute(low[1], "sp", forward)
         high_b = lax.ppermute(high[1], "sp", backward)
-        low_b = lax.ppermute(low[1], "sp", forward)
-        high_a = lax.ppermute(high[0], "sp", backward)
         return (low_a, low_b), (high_a, high_b)
 
     low, high = shift((kva, kvb), (kva, kvb))
@@ -396,12 +407,12 @@
     second_hop = [(i, i ^ (4 - 2 * (i % 2))) for i in range(n_tp)]
     low_edge = lax.ppermute(last_edge, "sp", forward[:-1])
     high_edge = lax.ppermute(first_edge, "sp", backward[:-1])
-    *state, w_own, lw_own = attend(q, [(kva, kvb), (low[0], high[1])], None, (grid_out_weight, local_out_weight))
+    *state, w_own, lw_own = attend(q, [(kva, kvb), (low[0], high[0])], None, (grid_out_weight, local_out_weight))
     w_other = lax.ppermute(w_own, "tp", flip)
     lw_other = lax.ppermute(lw_own, "tp", flip)
     for _ in range(1, (n_sp - 1) // 2):
         next_low, next_high = shift(low, high)
-        state = attend(q, [(low[1], high[0]), (next_low[0], next_high[1])], state)
+        state = attend(q, [(low[1], high[1]), (next_low[0], next_high[0])], state)
         low, high = next_low, next_high
     far = lax.ppermute(low[0], "sp", forward), lax.ppermute(high[1], "sp", backward)
 
@@ -416,7 +427,7 @@
         name="banded",
     )(sink_logit.reshape(1, heads), lq, lkv, low_edge, high_edge)
     lother = lax.ppermute(lsend, "tp", flip)
-    state = attend(q, [(low[1], high[0])], state)
+    state = attend(q, [(low[1], high[1])], state)
 
     piece = row_count // n_tp
     state = attend(q, [(far[0],)], state)
@@ -426,7 +437,24 @@
     other_rest = lax.ppermute(send_rest, "tp", flip)
 
     fixed = (lkeep, lother, w_own, lw_own, w_other, lw_other)
-    (pass_on,) = project((0,), (keep, other) + fixed, piece, bf16)
+    early = pl.pallas_call(
+        early_body,
+        out_shape=sds((piece, width), f32),
+        in_specs=vmem(6),
+        out_specs=vmem(1)[0],
+        compiler_params=params(8),
+        cost_estimate=cost(6 * piece * width * heads * HEAD),
+        name="early",
+    )(keep, lkeep, lother, w_own, lw_own, lw_other)
+    pass_on = pl.pallas_call(
+        pass_body,
+        out_shape=sds((piece, width), bf16),
+        in_specs=vmem(3),
+        out_specs=vmem(1)[0],
+        compiler_params=params(8),
+        cost_estimate=cost(2 * piece * width * heads * HEAD),
+        name="pass_on",
+    )(early, other, w_other)
     got_on = lax.ppermute(pass_on, "tp", first_hop)
     next_part, own_part = project((2, 3), (keep_rest, other_rest) + fixed, piece, f32)
     (direct,) = project((1,), (keep_rest, other_rest) + fixed, piece, bf16)

time: 69.8 us -> 69.7 us (level)
    ppermute x1, waiting for transfers between devices: 3.14 us -> 7.32 us  [shards(): low_edge = lax.ppermute(last_edge, 'sp', forward[:-1])]
    ppermute x1, waiting for transfers between devices: 3.99 us -> 0.01 us  [shift(): low_a = lax.ppermute(low[0], 'sp', forward)]
    ppermute x1, starting transfers between devices: 0.01 us -> 3.11 us  [shift(): low_a = lax.ppermute(low[0], 'sp', forward)]
    ppermute x1, starting transfers between devices: 5.12 us -> 2.32 us  [shift(): high_b = lax.ppermute(high[1], 'sp', backward)]
    ppermute x1, waiting for transfers between devices: 0.01 us -> 2.72 us  [shift(): high_a = lax.ppermute(high[0], 'sp', backward)]
    ppermute x1, waiting for transfers between devices: 2.55 us -> 0.01 us  [shift(): high_b = lax.ppermute(high[1], 'sp', backward)]
    ppermute x1, starting transfers between devices: 1.61 us -> 0.01 us  [shift(): low_b = lax.ppermute(low[1], 'sp', forward)]
    pallas_call x0 -> x2, Pallas kernels: none -> 0.94 us  [the longest x1 0.64 us: shards(): pl.pallas_call(early_body, out_shape=sds((piece, width), f32), in_specs=v...]
  transfers between devices with their start and end apart: 16 -> 16, of which waited for: 10 -> 10; matrix products, arithmetic and copies ran while one was open for 0% -> 0% of each run, Pallas kernels for 18% -> 23%
where the time goes in v2:
time: 69.7 us; the launch traced here: 69.3 us
  waiting for transfers between devices  25.6 us (37%)
  Pallas kernels  22.2 us (32%)
  starting transfers between devices  20.4 us (29%)
  other arithmetic  0.97 us (1%)
    ppermute x1, waiting for transfers between devices, shards(): low_edge = lax.ppermute(last_edge, 'sp', forward[:-1])  7.32 us
    pallas_call x3, Pallas kernels, attend(): pl.pallas_call(functools.partial(attend_body, 256, tuple((len(block) for...  6.62 us
    ppermute x1, waiting for transfers between devices, shards(): got = lax.ppermute(direct, 'tp', first_hop)  5.67 us
    ppermute x1, waiting for transfers between devices, shards(): high_edge = lax.ppermute(first_edge, 'sp', backward[:-1])  5.33 us
    ppermute x1, starting transfers between devices, shift(): low_a = lax.ppermute(low[0], 'sp', forward)  3.11 us
    pallas_call x1, Pallas kernels, shards(): pl.pallas_call(second_keys_body, out_shape=rows_out + tuple((sds(w.shape,...  3.01 us
    ppermute x1, starting transfers between devices, shards(): low_edge = lax.ppermute(last_edge, 'sp', forward[:-1])  2.74 us
    pallas_call x1, Pallas kernels, shards(): pl.pallas_call(q_body, out_shape=(sds((heads * row_count, HEAD), bf16), s...  2.72 us
  transfers between devices with their start and end apart: 16, of which 10 were waited for; matrix products, arithmetic and copies ran while one was open for 0% of the time, Pallas kernels for 23%

profile of v2, /device:TPU:0, one launch (start us, length us, event | category | flops | bytes accessed | tf_op | source)
XLA Modules:
  0.0 69.3 jit_solution(18329169601649502484)
XLA Ops:
  0.0 2.7 %keys_a.1 = (bf16[384,2048]{1,0:T(8,128)(2,1)S(1)}, bf16[384,256]{1,0:T(8,128)(2,1)S(1)}, bf16[384,2048]{1,0:T(8,128)(2,1)S(1)}, f32[1,2048]{1,0:T(1,128)S(1)}, ...) custom-call(bf16[768,2048]{1,0:T(8,128)(2,1)} %tok.1, ...), custom_call_target="tpu_custom_call" | custom-call | flops 120795952 | bytes 4194304 | tf_op jit(solution)/shard_map/keys_a/pallas_call | solution.py:355
  2.7 3.1 %collective-permute-start.2 = (bf16[384,256]{1,0:T(8,128)(2,1)S(1)}, bf16[384,256]{1,0:T(8,128)(2,1)S(1)}, u32[]{:S(2)}, u32[]{:S(2)}) collective-permute-start(bf16[384,256]{1,0:T(8,128)(2,1)S(1)} %get-tuple-element.58.refs_1_), channel_id=1, source_target_pairs={{0,8},{8,16},{16,24},{24,0},{1,9},{9,17},{17,25},{25,1},{2,10},{10... | collective-permute-start | bytes 589832 | tf_op jit(solution)/shard_map/ppermute | solution.py:381
  5.8 2.1 %collective-permute-start.5 = (bf16[384,256]{1,0:T(8,128)(2,1)S(1)}, bf16[384,256]{1,0:T(8,128)(2,1)S(1)}, u32[]{:S(2)}, u32[]{:S(2)}) collective-permute-start(bf16[384,256]{1,0:T(8,128)(2,1)S(1)} %get-tuple-element.58.refs_1_), channel_id=1, source_target_pairs={{8,0},{16,8},{24,16},{0,24},{9,1},{17,9},{25,17},{1,25},{10,2},{18... | collective-permute-start | bytes 589832 | tf_op jit(solution)/shard_map/ppermute | solution.py:382
  7.9 3.0 %keys_b.1 = (bf16[384,2048]{1,0:T(8,128)(2,1)S(1)}, bf16[384,256]{1,0:T(8,128)(2,1)S(1)}, bf16[2048,256]{1,0:T(8,128)(2,1)S(1)}, bf16[2048,256]{1,0:T(8,128)(2,1...) custom-call(bf16[384,2048]{1,0:T(8,128)(2,1)S(1)} %get-tuple-element.43.tok, ...), custom_call_target="tpu_custom_call" | custom-call | flops 120795952 | bytes 4194304 | tf_op jit(solution)/shard_map/keys_b/pallas_call | solution.py:365
  10.9 2.7 %queries.1 = (bf16[1536,128]{1,0:T(8,128)(2,1)S(1)}, bf16[768,256]{1,0:T(8,128)(2,1)S(1)}, bf16[768,256]{1,0:T(8,128)(2,1)S(1)}, bf16[128,256]{1,0:T(8,128)(2,1)S(1)}, bf16[128,256]{1,0:T(8,128)(2,1)S(1)}) custom-call(bf16[384,2048]{1,0:T(8,128)(2,1)S(1)} %get-tuple-element.42.normed_a, bf16[384,2048]{1,0:T(8,128)(2,1)S(1)} %get-tuple-element.50.normed_b, ...), custom_call_target="tpu_custom_call" | custom-call | flops 724775744 | bytes 6291456 | tf_op jit(solution)/shard_map/queries/pallas_call | solution.py:389
  13.6 0.0 collective-permute-done.2.refs_3_
  13.6 2.7 %collective-permute-done.5.refs_4_ = bf16[384,256]{1,0:T(8,128)(2,1)S(1)} collective-permute-done((bf16[384,256]{1,0:T(8,128)(2,1)S(1)}, bf16[384,256]{1,0:T(8,128)(2,1)S(1)}, u32[]{:S(2)}, u32[]{:S(2)}) %collective-permute-start.5) | collective-permute-done | bytes 196640 | tf_op jit(solution)/shard_map/ppermute | solution.py:382
  16.3 3.2 %shard_map.145 = (f32[1536,128]{1,0:T(8,128)S(1)}, f32[1536,256]{1,0:T(8,128)S(1)}, bf16[256,2048]{1,0:T(8,128)(2,1)S(1)}, bf16[256,2048]{1,0:T(8,128)(2,1)S(1)}) custom-call(bf16[1536,128]{1,0:T(8,128)(2,1)S(1)} %get-tuple-element.56.refs_0_.q, bf16[384,256]{1,0:T(8,128)(2,1)S(1)} %get-tuple-element.58.refs_1_, ...), custom_call_target="tpu_custom_call" | custom-call | flops 724775744 | tf_op jit(solution)/shard_map/pallas_call | solution.py:285
  19.5 0.1 collective-permute-start.11
  19.6 0.5 collective-permute-start.10
  20.1 2.3 %collective-permute-start = (bf16[384,256]{1,0:T(8,128)(2,1)S(1)}, bf16[384,256]{1,0:T(8,128)(2,1)S(1)}, u32[]{:S(2)}, u32[]{:S(2)}) collective-permute-start(bf16[384,256]{1,0:T(8,128)(2,1)S(1)} %get-tuple-element.57.refs_2_), channel_id=1, source_target_pairs={{8,0},{16,8},{24,16},{0,24},{9,1},{17,9},{25,17},{1,25},{10,2},{18... | collective-permute-start | bytes 589832 | tf_op jit(solution)/shard_map/ppermute | solution.py:384
  22.4 0.0 collective-permute-start.4
  22.4 2.7 %collective-permute-start.7 = (bf16[128,256]{1,0:T(8,128)(2,1)S(1)}, bf16[128,256]{1,0:T(8,128)(2,1)S(1)}, u32[]{:S(2)}, u32[]{:S(2)}) collective-permute-start(bf16[128,256]{1,0:T(8,128)(2,1)S(1)} %get-tuple-element.69), channel_id=1, source_target_pairs={{0,8},{8,16},{16,24},{1,9},{9,17},{17,25},{2,10},{10,18},{18,26},{... | collective-permute-start | bytes 196616 | tf_op jit(solution)/shard_map/ppermute | solution.py:408
  25.2 7.3 %collective-permute-done.7.low = bf16[128,256]{1,0:T(8,128)(2,1)S(1)} collective-permute-done((bf16[128,256]{1,0:T(8,128)(2,1)S(1)}, bf16[128,256]{1,0:T(8,128)(2,1)S(1)}, u32[]{:S(2)}, u32[]{:S(2)}) %collective-permute-start.7) | collective-permute-done | bytes 65568 | tf_op jit(solution)/shard_map/ppermute | solution.py:408
  32.5 1.3 %collective-permute-start.8 = (bf16[128,256]{1,0:T(8,128)(2,1)S(1)}, bf16[128,256]{1,0:T(8,128)(2,1)S(1)}, u32[]{:S(2)}, u32[]{:S(2)}) collective-permute-start(bf16[128,256]{1,0:T(8,128)(2,1)S(1)} %get-tuple-element.70), channel_id=1, source_target_pairs={{8,0},{16,8},{24,16},{9,1},{17,9},{25,17},{10,2},{18,10},{26,18},{... | collective-permute-start | bytes 196616 | tf_op jit(solution)/shard_map/ppermute | solution.py:409
  33.8 5.3 %collective-permute-done.8.high = bf16[128,256]{1,0:T(8,128)(2,1)S(1)} collective-permute-done((bf16[128,256]{1,0:T(8,128)(2,1)S(1)}, bf16[128,256]{1,0:T(8,128)(2,1)S(1)}, u32[]{:S(2)}, u32[]{:S(2)}) %collective-permute-start.8) | collective-permute-done | bytes 65568 | tf_op jit(solution)/shard_map/ppermute | solution.py:409
  39.1 2.0 %collective-permute-start.3 = (bf16[384,256]{1,0:T(8,128)(2,1)S(1)}, bf16[384,256]{1,0:T(8,128)(2,1)S(1)}, u32[]{:S(2)}, u32[]{:S(2)}) collective-permute-start(bf16[384,256]{1,0:T(8,128)(2,1)S(1)} %collective-permute-done.2.refs_3_), channel_id=1, source_target_pairs={{0,8},{8,16},{16,24},{24,0},{1,9},{9,17},{17,25},{25,1},{2,10},{10... | collective-permute-start | bytes 589832 | tf_op jit(solution)/shard_map/ppermute | solution.py:417
  41.1 0.0 collective-permute-done.refs_2_
  41.1 1.8 %collective-permute-start.1 = (bf16[384,256]{1,0:T(8,128)(2,1)S(1)}, bf16[384,256]{1,0:T(8,128)(2,1)S(1)}, u32[]{:S(2)}, u32[]{:S(2)}) collective-permute-start(bf16[384,256]{1,0:T(8,128)(2,1)S(1)} %collective-permute-done.refs_2_), channel_id=1, source_target_pairs={{8,0},{16,8},{24,16},{0,24},{9,1},{17,9},{25,17},{1,25},{10,2},{18... | collective-permute-start | bytes 589832 | tf_op jit(solution)/shard_map/ppermute | solution.py:417
  43.0 2.1 %banded.1 = (bf16[384,256]{1,0:T(8,128)(2,1)S(1)}, bf16[384,256]{1,0:T(8,128)(2,1)S(1)}) custom-call(f32[1,2]{1,0:T(1,128)S(1)} %bitcast.4, bf16[768,256]{1,0:T(8,128)(2,1)S(1)} %get-tuple-element.67.lq, bf16[768,256]{1,0:T(8,128)(2,1)S(1)} %get-tuple-element.68.lkv, bf16[128,256]{1,0:T(8,128)(2,1)S(1)} %collective-permute-done.7.low, ...), custom_call_target="tpu_custom_call" | custom-call | flops 181193936 | tf_op jit(solution)/shard_map/banded/pallas_call | solution.py:419
  45.0 0.0 collective-permute-done.4.refs_1_
  45.1 0.1 collective-permute-start.9
  45.1 1.9 %shard_map.146 = (f32[1536,128]{1,0:T(8,128)S(1)}, f32[1536,256]{1,0:T(8,128)S(1)}) custom-call(bf16[1536,128]{1,0:T(8,128)(2,1)S(1)} %get-tuple-element.56.refs_0_.q, bf16[384,256]{1,0:T(8,128)(2,1)S(1)} %collective-permute-done.4.refs_1_, bf16[384,256]{1,0:T(8,128)(2,1)S(1)} %collective-permute-done.refs_2_, f32[1536,128]{1,0:T(8,128)S(1)} %get-tuple-element.59.refs_3_, ...), custom_call_target="tpu_custom_call" | custom-call | flops 362387872 | tf_op jit(solution)/shard_map/pallas_call | solution.py:285
  47.0 1.2 %collective-permute-done.3.refs_1_ = bf16[384,256]{1,0:T(8,128)(2,1)S(1)} collective-permute-done((bf16[384,256]{1,0:T(8,128)(2,1)S(1)}, bf16[384,256]{1,0:T(8,128)(2,1)S(1)}, u32[]{:S(2)}, u32[]{:S(2)}) %collective-permute-start.3) | collective-permute-done | bytes 196640 | tf_op jit(solution)/shard_map/ppermute | solution.py:417
  48.2 1.6 %shard_map.147 = (f32[1536,128]{1,0:T(8,128)S(1)}, f32[1536,256]{1,0:T(8,128)S(1)}) custom-call(bf16[1536,128]{1,0:T(8,128)(2,1)S(1)} %get-tuple-element.56.refs_0_.q, bf16[384,256]{1,0:T(8,128)(2,1)S(1)} %collective-permute-done.3.refs_1_, f32[1536,128]{1,0:T(8,128)S(1)} %get-tuple-element.61.refs_2_, f32[1536,256]{1,0:T(8,128)S(1)} %get-tuple-element.62.refs_3_), custom_call_target="tpu_custom_call" | custom-call | flops 181193936 | tf_op jit(solution)/shard_map/pallas_call | solution.py:285
  49.8 0.1 collective-permute-done.1.kv
  49.9 0.6 shard_map.151
  50.5 0.1 collective-permute-start.13
  50.6 0.0 collective-permute-done.9.lother
  50.6 0.0 collective-permute-done.11.lw_other
  50.6 0.6 early.1
  51.3 0.6 collective-permute-done.13.other
  51.8 0.0 collective-permute-done.10.w_other
  51.8 0.3 pass_on.1
  52.1 1.5 %collective-permute-start.14 = (bf16[96,2048]{1,0:T(8,128)(2,1)S(1)}, bf16[96,2048]{1,0:T(8,128)(2,1)S(1)}, u32[]{:S(2)}, u32[]{:S(2)}) collective-permute-start(bf16[96,2048]{1,0:T(8,128)(2,1)S(1)} %pass_on.1), channel_id=1, source_target_pairs={{0,2},{1,5},{2,0},{3,7},{4,6},{5,1},{6,4},{7,3},{8,10},{9,13},{10,... | collective-permute-start | bytes 1179656 | tf_op jit(solution)/shard_map/ppermute | solution.py:458
  53.7 1.4 %shard_map.148 = (bf16[288,256]{1,0:T(8,128)(2,1)S(1)}, bf16[288,256]{1,0:T(8,128)(2,1)S(1)}) custom-call(bf16[1536,128]{1,0:T(8,128)(2,1)S(1)} %get-tuple-element.56.refs_0_.q, bf16[384,256]{1,0:T(8,128)(2,1)S(1)} %collective-permute-done.1.kv, f32[1536,128]{1,0:T(8,128)S(1)} %get-tuple-element.63.m_in, f32[1536,256]{1,0:T(8,128)S(1)} %get-tuple-element.64.acc_in), custom_call_target="tpu_custom_call" | custom-call | flops 135895456 | tf_op jit(solution)/shard_map/pallas_call | solution.py:300
  55.0 0.1 collective-permute-start.6
  55.1 1.4 %collective-permute-done.6.other = bf16[288,256]{1,0:T(8,128)(2,1)S(1)} collective-permute-done((bf16[288,256]{1,0:T(8,128)(2,1)S(1)}, bf16[288,256]{1,0:T(8,128)(2,1)S(1)}, u32[]{:S(2)}, u32[]{:S(2)}) %collective-permute-start.6) | collective-permute-done | bytes 147488 | tf_op jit(solution)/shard_map/ppermute | solution.py:437
  56.5 0.8 %shard_map.150 = bf16[96,2048]{1,0:T(8,128)(2,1)S(1)} custom-call(bf16[288,256]{1,0:T(8,128)(2,1)S(1)} %get-tuple-element.65.keep, bf16[288,256]{1,0:T(8,128)(2,1)S(1)} %collective-permute-done.6.other, bf16[384,256]{1,0:T(8,128)(2,1)S(1)} %get-tuple-element.71.lkeep, bf16[384,256]{1,0:T(8,128)(2,1)S(1)} %collective-permute-done.9.lother, ...), custom_call_target="tpu_custom_call" | custom-call | flops 120795952 | bytes 4194304 | tf_op jit(solution)/shard_map/pallas_call | solution.py:313
  57.3 1.1 %collective-permute-start.12 = (bf16[96,2048]{1,0:T(8,128)(2,1)S(1)}, bf16[96,2048]{1,0:T(8,128)(2,1)S(1)}, u32[]{:S(2)}, u32[]{:S(2)}) collective-permute-start(bf16[96,2048]{1,0:T(8,128)(2,1)S(1)} %shard_map.150), channel_id=1, source_target_pairs={{0,2},{1,5},{2,0},{3,7},{4,6},{5,1},{6,4},{7,3},{8,10},{9,13},{10,... | collective-permute-start | bytes 1179656 | tf_op jit(solution)/shard_map/ppermute | solution.py:461
  58.4 1.4 %shard_map.149 = (f32[96,2048]{1,0:T(8,128)S(1)}, f32[96,2048]{1,0:T(8,128)S(1)}) custom-call(bf16[288,256]{1,0:T(8,128)(2,1)S(1)} %get-tuple-element.65.keep, bf16[288,256]{1,0:T(8,128)(2,1)S(1)} %collective-permute-done.6.other, bf16[384,256]{1,0:T(8,128)(2,1)S(1)} %get-tuple-element.71.lkeep, bf16[384,256]{1,0:T(8,128)(2,1)S(1)} %collective-permute-done.9.lother, ...), custom_call_target="tpu_custom_call" | custom-call | flops 241591904 | bytes 4194304 | tf_op jit(solution)/shard_map/pallas_call | solution.py:313
  59.8 0.1 collective-permute-done.14
  60.0 0.1 add_convert_fusion.1
  60.1 1.6 %collective-permute-start.15 = (bf16[96,2048]{1,0:T(8,128)(2,1)S(1)}, bf16[96,2048]{1,0:T(8,128)(2,1)S(1)}, u32[]{:S(2)}, u32[]{:S(2)}) collective-permute-start(bf16[96,2048]{1,0:T(8,128)(2,1)S(1)} %add_convert_fusion.1), channel_id=1, source_target_pairs={{0,4},{1,3},{2,6},{3,1},{4,0},{5,7},{6,2},{7,5},{8,12},{9,11},{10,... | collective-permute-start | bytes 1179656 | tf_op jit(solution)/shard_map/ppermute | solution.py:462
  61.6 5.7 %collective-permute-done.12 = bf16[96,2048]{1,0:T(8,128)(2,1)S(1)} collective-permute-done((bf16[96,2048]{1,0:T(8,128)(2,1)S(1)}, bf16[96,2048]{1,0:T(8,128)(2,1)S(1)}, u32[]{:S(2)}, u32[]{:S(2)}) %collective-permute-start.12) | collective-permute-done | bytes 393248 | tf_op jit(solution)/shard_map/ppermute | solution.py:461
  67.3 0.1 convert_add_fusion
  67.4 1.1 %collective-permute-done.15 = bf16[96,2048]{1,0:T(8,128)(2,1)S(1)} collective-permute-done((bf16[96,2048]{1,0:T(8,128)(2,1)S(1)}, bf16[96,2048]{1,0:T(8,128)(2,1)S(1)}, u32[]{:S(2)}, u32[]{:S(2)}) %collective-permute-start.15) | collective-permute-done | bytes 393248 | tf_op jit(solution)/shard_map/ppermute | solution.py:462
  68.5 0.8 %add_convert_fusion = bf16[96,2048]{1,0:T(8,128)(2,1)} fusion(f32[96,2048]{1,0:T(8,128)S(1)} %convert_add_fusion, bf16[96,2048]{1,0:T(8,128)(2,1)S(1)} %collective-permute-done.15), kind=kLoop, calls=%fused_computation | loop fusion | flops 589824 | bytes 1572864 | tf_op jit(solution)/shard_map/convert_element_type | solution.py:464
  (2 shorter events, 0.0 us)
Async XLA Ops:
  2.7 11.0 %collective-permute-start.2 = (bf16[384,256]{1,0:T(8,128)(2,1)S(1)}, bf16[384,256]{1,0:T(8,128)(2,1)S(1)}, u32[]{:S(2)}, u32[]{:S(2)}) collective-permute-start(bf16[384,256]{1,0:T(8,128)(2,1)S(1)} %get-tuple-element.58.refs_1_), channel_id=1, source_target_pairs={{0,8},{8,16},{16,24},{24,0},{1,9},{9,17},{17,25},{25,1},{2,10},{10... | collective-permute-start | bytes 589832 | tf_op jit(solution)/shard_map/ppermute | solution.py:381
  5.8 10.6 %collective-permute-start.5 = (bf16[384,256]{1,0:T(8,128)(2,1)S(1)}, bf16[384,256]{1,0:T(8,128)(2,1)S(1)}, u32[]{:S(2)}, u32[]{:S(2)}) collective-permute-start(bf16[384,256]{1,0:T(8,128)(2,1)S(1)} %get-tuple-element.58.refs_1_), channel_id=1, source_target_pairs={{8,0},{16,8},{24,16},{0,24},{9,1},{17,9},{25,17},{1,25},{10,2},{18... | collective-permute-start | bytes 589832 | tf_op jit(solution)/shard_map/ppermute | solution.py:382
  16.3 26.6 %copy-start = (f32[2]{0:T(128)S(1)}, f32[2]{0:T(128)}, u32[]{:S(2)}) copy-start(f32[2]{0:T(128)} %param.25) | copy-start | bytes 28
  19.5 31.1 %collective-permute-start.11 = (bf16[256,2048]{1,0:T(8,128)(2,1)S(1)}, bf16[256,2048]{1,0:T(8,128)(2,1)S(1)}, u32[]{:S(2)}, u32[]{:S(2)}) collective-permute-start(bf16[256,2048]{1,0:T(8,128)(2,1)S(1)} %get-tuple-element.74.lw), channel_id=1, source_target_pairs={{0,1},{1,0},{2,3},{3,2},{4,5},{5,4},{6,7},{7,6},{8,9},{9,8},{10,11... | collective-permute-start | bytes 3145736 | tf_op jit(solution)/shard_map/ppermute | solution.py:412
  19.6 32.2 %collective-permute-start.10 = (bf16[256,2048]{1,0:T(8,128)(2,1)S(1)}, bf16[256,2048]{1,0:T(8,128)(2,1)S(1)}, u32[]{:S(2)}, u32[]{:S(2)}) collective-permute-start(bf16[256,2048]{1,0:T(8,128)(2,1)S(1)} %get-tuple-element.73.w), channel_id=1, source_target_pairs={{0,1},{1,0},{2,3},{3,2},{4,5},{5,4},{6,7},{7,6},{8,9},{9,8},{10,11... | collective-permute-start | bytes 3145736 | tf_op jit(solution)/shard_map/ppermute | solution.py:411
  20.1 21.0 %collective-permute-start = (bf16[384,256]{1,0:T(8,128)(2,1)S(1)}, bf16[384,256]{1,0:T(8,128)(2,1)S(1)}, u32[]{:S(2)}, u32[]{:S(2)}) collective-permute-start(bf16[384,256]{1,0:T(8,128)(2,1)S(1)} %get-tuple-element.57.refs_2_), channel_id=1, source_target_pairs={{8,0},{16,8},{24,16},{0,24},{9,1},{17,9},{25,17},{1,25},{10,2},{18... | collective-permute-start | bytes 589832 | tf_op jit(solution)/shard_map/ppermute | solution.py:384
  22.4 22.6 %collective-permute-start.4 = (bf16[384,256]{1,0:T(8,128)(2,1)S(1)}, bf16[384,256]{1,0:T(8,128)(2,1)S(1)}, u32[]{:S(2)}, u32[]{:S(2)}) collective-permute-start(bf16[384,256]{1,0:T(8,128)(2,1)S(1)} %get-tuple-element.57.refs_2_), channel_id=1, source_target_pairs={{0,8},{8,16},{16,24},{24,0},{1,9},{9,17},{17,25},{25,1},{2,10},{10... | collective-permute-start | bytes 589832 | tf_op jit(solution)/shard_map/ppermute | solution.py:383
  22.4 10.1 %collective-permute-start.7 = (bf16[128,256]{1,0:T(8,128)(2,1)S(1)}, bf16[128,256]{1,0:T(8,128)(2,1)S(1)}, u32[]{:S(2)}, u32[]{:S(2)}) collective-permute-start(bf16[128,256]{1,0:T(8,128)(2,1)S(1)} %get-tuple-element.69), channel_id=1, source_target_pairs={{0,8},{8,16},{16,24},{1,9},{9,17},{17,25},{2,10},{10,18},{18,26},{... | collective-permute-start | bytes 196616 | tf_op jit(solution)/shard_map/ppermute | solution.py:408
  32.5 6.6 %collective-permute-start.8 = (bf16[128,256]{1,0:T(8,128)(2,1)S(1)}, bf16[128,256]{1,0:T(8,128)(2,1)S(1)}, u32[]{:S(2)}, u32[]{:S(2)}) collective-permute-start(bf16[128,256]{1,0:T(8,128)(2,1)S(1)} %get-tuple-element.70), channel_id=1, source_target_pairs={{8,0},{16,8},{24,16},{9,1},{17,9},{25,17},{10,2},{18,10},{26,18},{... | collective-permute-start | bytes 196616 | tf_op jit(solution)/shard_map/ppermute | solution.py:409
  39.1 9.1 %collective-permute-start.3 = (bf16[384,256]{1,0:T(8,128)(2,1)S(1)}, bf16[384,256]{1,0:T(8,128)(2,1)S(1)}, u32[]{:S(2)}, u32[]{:S(2)}) collective-permute-start(bf16[384,256]{1,0:T(8,128)(2,1)S(1)} %collective-permute-done.2.refs_3_), channel_id=1, source_target_pairs={{0,8},{8,16},{16,24},{24,0},{1,9},{9,17},{17,25},{25,1},{2,10},{10... | collective-permute-start | bytes 589832 | tf_op jit(solution)/shard_map/ppermute | solution.py:417
  41.1 8.8 %collective-permute-start.1 = (bf16[384,256]{1,0:T(8,128)(2,1)S(1)}, bf16[384,256]{1,0:T(8,128)(2,1)S(1)}, u32[]{:S(2)}, u32[]{:S(2)}) collective-permute-start(bf16[384,256]{1,0:T(8,128)(2,1)S(1)} %collective-permute-done.refs_2_), channel_id=1, source_target_pairs={{8,0},{16,8},{24,16},{0,24},{9,1},{17,9},{25,17},{1,25},{10,2},{18... | collective-permute-start | bytes 589832 | tf_op jit(solution)/shard_map/ppermute | solution.py:417
  45.1 5.6 %collective-permute-start.9 = (bf16[384,256]{1,0:T(8,128)(2,1)S(1)}, bf16[384,256]{1,0:T(8,128)(2,1)S(1)}, u32[]{:S(2)}, u32[]{:S(2)}) collective-permute-start(bf16[384,256]{1,0:T(8,128)(2,1)S(1)} %get-tuple-element.72), channel_id=1, source_target_pairs={{0,1},{1,0},{2,3},{3,2},{4,5},{5,4},{6,7},{7,6},{8,9},{9,8},{10,11... | collective-permute-start | bytes 589832 | tf_op jit(solution)/shard_map/ppermute | solution.py:429
  50.5 1.3 %collective-permute-start.13 = (bf16[96,256]{1,0:T(8,128)(2,1)S(1)}, bf16[96,256]{1,0:T(8,128)(2,1)S(1)}, u32[]{:S(2)}, u32[]{:S(2)}) collective-permute-start(bf16[96,256]{1,0:T(8,128)(2,1)S(1)} %get-tuple-element.78), channel_id=1, source_target_pairs={{0,1},{1,0},{2,3},{3,2},{4,5},{5,4},{6,7},{7,6},{8,9},{9,8},{10,11... | collective-permute-start | bytes 147464 | tf_op jit(solution)/shard_map/ppermute | solution.py:435
  52.1 7.8 %collective-permute-start.14 = (bf16[96,2048]{1,0:T(8,128)(2,1)S(1)}, bf16[96,2048]{1,0:T(8,128)(2,1)S(1)}, u32[]{:S(2)}, u32[]{:S(2)}) collective-permute-start(bf16[96,2048]{1,0:T(8,128)(2,1)S(1)} %pass_on.1), channel_id=1, source_target_pairs={{0,2},{1,5},{2,0},{3,7},{4,6},{5,1},{6,4},{7,3},{8,10},{9,13},{10,... | collective-permute-start | bytes 1179656 | tf_op jit(solution)/shard_map/ppermute | solution.py:458
  55.0 1.4 %collective-permute-start.6 = (bf16[288,256]{1,0:T(8,128)(2,1)S(1)}, bf16[288,256]{1,0:T(8,128)(2,1)S(1)}, u32[]{:S(2)}, u32[]{:S(2)}) collective-permute-start(bf16[288,256]{1,0:T(8,128)(2,1)S(1)} %get-tuple-element.66), channel_id=1, source_target_pairs={{0,1},{1,0},{2,3},{3,2},{4,5},{5,4},{6,7},{7,6},{8,9},{9,8},{10,11... | collective-permute-start | bytes 442376 | tf_op jit(solution)/shard_map/ppermute | solution.py:437
  57.3 10.0 %collective-permute-start.12 = (bf16[96,2048]{1,0:T(8,128)(2,1)S(1)}, bf16[96,2048]{1,0:T(8,128)(2,1)S(1)}, u32[]{:S(2)}, u32[]{:S(2)}) collective-permute-start(bf16[96,2048]{1,0:T(8,128)(2,1)S(1)} %shard_map.150), channel_id=1, source_target_pairs={{0,2},{1,5},{2,0},{3,7},{4,6},{5,1},{6,4},{7,3},{8,10},{9,13},{10,... | collective-permute-start | bytes 1179656 | tf_op jit(solution)/shard_map/ppermute | solution.py:461
  60.1 8.5 %collective-permute-start.15 = (bf16[96,2048]{1,0:T(8,128)(2,1)S(1)}, bf16[96,2048]{1,0:T(8,128)(2,1)S(1)}, u32[]{:S(2)}, u32[]{:S(2)}) collective-permute-start(bf16[96,2048]{1,0:T(8,128)(2,1)S(1)} %add_convert_fusion.1), channel_id=1, source_target_pairs={{0,4},{1,3},{2,6},{3,1},{4,0},{5,7},{6,2},{7,5},{8,12},{9,11},{10,... | collective-permute-start | bytes 1179656 | tf_op jit(solution)/shard_map/ppermute | solution.py:462

commit v3 on v2

--- a/solution.py
+++ b/solution.py
@@ -90,29 +90,33 @@
 
 
 def first_keys_body(tile, tok, gain, kgain, row_tab, col_tab, wk, wv,
-                    normed, kv, tok_b, gain_v, kgain_v, row_v, col_v, wk_v, wv_v, tok_v, sems):
+                    normed, kv, gain_v, kgain_v, row_v, col_v, wk_v, wv_v, tok_v, sems):
     half = normed.shape[0]
     rows = [pl.ds(i, tile) for i in range(0, half, tile)]
     pairs = [(gain, gain_v)] + [(tok.at[r], tok_v.at[r]) for r in rows] + [(wk, wk_v), (wv, wv_v)]
     pairs += [(kgain, kgain_v), (row_tab.at[place()[0]], row_v), (col_tab, col_v)]
-    copies = start_copies(pairs + [(tok.at[pl.ds(half, half)], tok_b)], sems)
+    copies = start_copies(pairs, sems)
     copies[0].wait()
     for r, copy in zip(rows, copies[1:]):
         copy.wait()
         normed[r, :] = norm_rows(tok_v[r, :], gain_v[...])
-    for copy in copies[1 + len(rows) : -1]:
+    for copy in copies[1 + len(rows) :]:
         copy.wait()
     kv_rows(0, normed, wk_v, wv_v, kgain_v, row_v, col_v, kv)
-    copies[-1].wait()
-
-
-def second_keys_body(tok, gain, kgain, row_tab, col_tab, wk, wv, wq, lwq, lwk, lwv, qgain,
-                     normed, kv, wq_v, lwq_v, lwk_v, lwv_v, qgain_v, sems):
-    pairs = [(wq, wq_v), (lwq, lwq_v), (lwk, lwk_v), (lwv, lwv_v), (qgain, qgain_v)]
+
+
+def second_keys_body(tile, gain, kgain, row_tab, col_tab, wk, wv, tok, wq, lwq, lwk, lwv, qgain,
+                     normed, kv, wq_v, lwq_v, lwk_v, lwv_v, qgain_v, tok_v, sems):
+    half = normed.shape[0]
+    rows = [pl.ds(i, tile) for i in range(0, half, tile)]
+    pairs = [(tok.at[pl.ds(half + r.start, tile)], tok_v.at[r]) for r in rows]
+    pairs += [(wq, wq_v), (lwq, lwq_v), (lwk, lwk_v), (lwv, lwv_v), (qgain, qgain_v)]
     copies = start_copies(pairs, sems)
-    normed[...] = norm_rows(tok[...], gain[...])
-    kv_rows(normed.shape[0], normed, wk, wv, kgain, row_tab, col_tab, kv)
-    for copy in copies:
+    for r, copy in zip(rows, copies):
+        copy.wait()
+        normed[r, :] = norm_rows(tok_v[r, :], gain[...])
+    kv_rows(half, normed, wk, wv, kgain, row_tab, col_tab, kv)
+    for copy in copies[len(rows) :]:
         copy.wait()
 
 
@@ -352,26 +356,26 @@
     query_weights = grid_query_weight, local_query_weight, local_key_weight, local_value_weight
     rows_out = sds((half, width), bf16), sds((half, 2 * HEAD), bf16)
     key_cost = cost(2 * half * width * 2 * HEAD, 0, 4 * MIB)
-    normed_a, kva, tokens_b, *shared = pl.pallas_call(
+    normed_a, kva, *shared = pl.pallas_call(
         functools.partial(first_keys_body, tile),
-        out_shape=rows_out + (sds((half, width), bf16),) + tables + tuple(sds(w.shape, bf16) for w in key_weights),
+        out_shape=rows_out + tables + tuple(sds(w.shape, bf16) for w in key_weights),
         in_specs=hbm(7),
-        out_specs=tuple(vmem(9)),
-        scratch_shapes=[pltpu.VMEM((half, width), bf16), pltpu.SemaphoreType.DMA((7 + half // tile,))],
+        out_specs=tuple(vmem(8)),
+        scratch_shapes=[pltpu.VMEM((half, width), bf16), pltpu.SemaphoreType.DMA((6 + half // tile,))],
         compiler_params=params(16),
         cost_estimate=key_cost,
         name="keys_a",
     )(*in_hbm(tokens, norm_gain.reshape(1, width), grid_key_gain.reshape(1, HEAD), row_tab, col_tab, *key_weights))
     normed_b, kvb, *held = pl.pallas_call(
-        second_keys_body,
+        functools.partial(second_keys_body, tile),
         out_shape=rows_out + tuple(sds(w.shape, bf16) for w in query_weights) + (sds((1, HEAD), f32),),
-        in_specs=vmem(7) + hbm(5),
+        in_specs=vmem(6) + hbm(6),
         out_specs=tuple(vmem(7)),
-        scratch_shapes=[pltpu.SemaphoreType.DMA((5,))],
+        scratch_shapes=[pltpu.VMEM((half, width), bf16), pltpu.SemaphoreType.DMA((5 + half // tile,))],
         compiler_params=params(16),
         cost_estimate=key_cost,
         name="keys_b",
-    )(tokens_b, *shared, *in_hbm(*query_weights, grid_query_gain.reshape(1, HEAD)))
+    )(*shared, *in_hbm(tokens, *query_weights, grid_query_gain.reshape(1, HEAD)))
 
     forward = [(i, (i + 1) % n_sp) for i in range(n_sp)]
     backward = [(t, s) for s, t in forward]
@@ -460,7 +464,7 @@
     (direct,) = project((1,), (keep_rest, other_rest) + fixed, piece, bf16)
     got = lax.ppermute(direct, "tp", first_hop)
     got_next = lax.ppermute((next_part + got_on.astype(f32)).astype(bf16), "tp", second_hop)
-    summed = lax.optimization_barrier(own_part + got.astype(f32))
+    summed = own_part + got.astype(f32)
     return (summed + got_next.astype(f32)).astype(bf16)
 
 

time: 69.7 us -> 69.8 us (level)
  transfers between devices with their start and end apart: 16 -> 16, of which waited for: 10 -> 11; matrix products, arithmetic and copies ran while one was open for 0% -> 0% of each run, Pallas kernels for 23% -> 22%
where the time goes in v3:
time: 69.8 us; the launch traced here: 69.4 us
  waiting for transfers between devices  26.2 us (38%)
  Pallas kernels  21.7 us (31%)
  starting transfers between devices  20.4 us (29%)
  other arithmetic  0.94 us (1%)
    ppermute x1, waiting for transfers between devices, shards(): low_edge = lax.ppermute(last_edge, 'sp', forward[:-1])  7.32 us
    pallas_call x3, Pallas kernels, attend(): pl.pallas_call(functools.partial(attend_body, 256, tuple((len(block) for...  6.6 us
    ppermute x1, waiting for transfers between devices, shards(): got = lax.ppermute(direct, 'tp', first_hop)  5.68 us
    ppermute x1, waiting for transfers between devices, shards(): high_edge = lax.ppermute(first_edge, 'sp', backward[:-1])  5.33 us
    ppermute x1, starting transfers between devices, shift(): low_a = lax.ppermute(low[0], 'sp', forward)  3.11 us
    ppermute x1, waiting for transfers between devices, shift(): high_a = lax.ppermute(high[0], 'sp', backward)  2.75 us
    ppermute x1, starting transfers between devices, shards(): low_edge = lax.ppermute(last_edge, 'sp', forward[:-1])  2.74 us
    pallas_call x1, Pallas kernels, shards(): pl.pallas_call(q_body, out_shape=(sds((heads * row_count, HEAD), bf16), s...  2.71 us
  transfers between devices with their start and end apart: 16, of which 11 were waited for; matrix products, arithmetic and copies ran while one was open for 0% of the time, Pallas kernels for 22%

profile of v3, /device:TPU:0, one launch (start us, length us, event | category | flops | bytes accessed | tf_op | source)
XLA Modules:
  0.0 69.4 jit_solution(17574984086177723544)
XLA Ops:
  0.0 2.7 %keys_a.1 = (bf16[384,2048]{1,0:T(8,128)(2,1)S(1)}, bf16[384,256]{1,0:T(8,128)(2,1)S(1)}, f32[1,2048]{1,0:T(1,128)S(1)}, f32[1,128]{1,0:T(1,128)S(1)}, f32[3,12,...) custom-call(bf16[768,2048]{1,0:T(8,128)(2,1)} %tok.3, ...), custom_call_target="tpu_custom_call" | custom-call | flops 120795952 | bytes 4194304 | tf_op jit(solution)/shard_map/keys_a/pallas_call | solution.py:359
  2.7 3.1 %collective-permute-start.2 = (bf16[384,256]{1,0:T(8,128)(2,1)S(1)}, bf16[384,256]{1,0:T(8,128)(2,1)S(1)}, u32[]{:S(2)}, u32[]{:S(2)}) collective-permute-start(bf16[384,256]{1,0:T(8,128)(2,1)S(1)} %get-tuple-element.56.refs_1_), channel_id=1, source_target_pairs={{0,8},{8,16},{16,24},{24,0},{1,9},{9,17},{17,25},{25,1},{2,10},{10... | collective-permute-start | bytes 589832 | tf_op jit(solution)/shard_map/ppermute | solution.py:385
  5.8 2.1 %collective-permute-start.5 = (bf16[384,256]{1,0:T(8,128)(2,1)S(1)}, bf16[384,256]{1,0:T(8,128)(2,1)S(1)}, u32[]{:S(2)}, u32[]{:S(2)}) collective-permute-start(bf16[384,256]{1,0:T(8,128)(2,1)S(1)} %get-tuple-element.56.refs_1_), channel_id=1, source_target_pairs={{8,0},{16,8},{24,16},{0,24},{9,1},{17,9},{25,17},{1,25},{10,2},{18... | collective-permute-start | bytes 589832 | tf_op jit(solution)/shard_map/ppermute | solution.py:386
  7.9 2.5 %keys_b.1 = (bf16[384,2048]{1,0:T(8,128)(2,1)S(1)}, bf16[384,256]{1,0:T(8,128)(2,1)S(1)}, bf16[2048,256]{1,0:T(8,128)(2,1)S(1)}, bf16[2048,256]{1,0:T(8,128)(2,1...) custom-call(f32[1,2048]{1,0:T(1,128)S(1)} %get-tuple-element.42.gain, ...), custom_call_target="tpu_custom_call" | custom-call | flops 120795952 | bytes 4194304 | tf_op jit(solution)/shard_map/keys_b/pallas_call | solution.py:369
  10.4 2.7 %queries.1 = (bf16[1536,128]{1,0:T(8,128)(2,1)S(1)}, bf16[768,256]{1,0:T(8,128)(2,1)S(1)}, bf16[768,256]{1,0:T(8,128)(2,1)S(1)}, bf16[128,256]{1,0:T(8,128)(2,1)S(1)}, bf16[128,256]{1,0:T(8,128)(2,1)S(1)}) custom-call(bf16[384,2048]{1,0:T(8,128)(2,1)S(1)} %get-tuple-element.41.normed_a, bf16[384,2048]{1,0:T(8,128)(2,1)S(1)} %get-tuple-element.48.normed_b, ...), custom_call_target="tpu_custom_call" | custom-call | flops 724775744 | bytes 6291456 | tf_op jit(solution)/shard_map/queries/pallas_call | solution.py:393
  13.1 0.5 collective-permute-done.2.refs_3_
  13.6 2.8 %collective-permute-done.5.refs_4_ = bf16[384,256]{1,0:T(8,128)(2,1)S(1)} collective-permute-done((bf16[384,256]{1,0:T(8,128)(2,1)S(1)}, bf16[384,256]{1,0:T(8,128)(2,1)S(1)}, u32[]{:S(2)}, u32[]{:S(2)}) %collective-permute-start.5) | collective-permute-done | bytes 196640 | tf_op jit(solution)/shard_map/ppermute | solution.py:386
  16.3 3.2 %shard_map.145 = (f32[1536,128]{1,0:T(8,128)S(1)}, f32[1536,256]{1,0:T(8,128)S(1)}, bf16[256,2048]{1,0:T(8,128)(2,1)S(1)}, bf16[256,2048]{1,0:T(8,128)(2,1)S(1)}) custom-call(bf16[1536,128]{1,0:T(8,128)(2,1)S(1)} %get-tuple-element.54.refs_0_.q, bf16[384,256]{1,0:T(8,128)(2,1)S(1)} %get-tuple-element.56.refs_1_, ...), custom_call_target="tpu_custom_call" | custom-call | flops 724775744 | tf_op jit(solution)/shard_map/pallas_call | solution.py:289
  19.5 0.1 collective-permute-start.11
  19.6 0.5 collective-permute-start.10
  20.1 2.3 %collective-permute-start = (bf16[384,256]{1,0:T(8,128)(2,1)S(1)}, bf16[384,256]{1,0:T(8,128)(2,1)S(1)}, u32[]{:S(2)}, u32[]{:S(2)}) collective-permute-start(bf16[384,256]{1,0:T(8,128)(2,1)S(1)} %get-tuple-element.55.refs_2_), channel_id=1, source_target_pairs={{8,0},{16,8},{24,16},{0,24},{9,1},{17,9},{25,17},{1,25},{10,2},{18... | collective-permute-start | bytes 589832 | tf_op jit(solution)/shard_map/ppermute | solution.py:388
  22.4 0.0 collective-permute-start.4
  22.4 2.7 %collective-permute-start.7 = (bf16[128,256]{1,0:T(8,128)(2,1)S(1)}, bf16[128,256]{1,0:T(8,128)(2,1)S(1)}, u32[]{:S(2)}, u32[]{:S(2)}) collective-permute-start(bf16[128,256]{1,0:T(8,128)(2,1)S(1)} %get-tuple-element.67), channel_id=1, source_target_pairs={{0,8},{8,16},{16,24},{1,9},{9,17},{17,25},{2,10},{10,18},{18,26},{... | collective-permute-start | bytes 196616 | tf_op jit(solution)/shard_map/ppermute | solution.py:412
  25.2 7.3 %collective-permute-done.7.low = bf16[128,256]{1,0:T(8,128)(2,1)S(1)} collective-permute-done((bf16[128,256]{1,0:T(8,128)(2,1)S(1)}, bf16[128,256]{1,0:T(8,128)(2,1)S(1)}, u32[]{:S(2)}, u32[]{:S(2)}) %collective-permute-start.7) | collective-permute-done | bytes 65568 | tf_op jit(solution)/shard_map/ppermute | solution.py:412
  32.5 1.3 %collective-permute-start.8 = (bf16[128,256]{1,0:T(8,128)(2,1)S(1)}, bf16[128,256]{1,0:T(8,128)(2,1)S(1)}, u32[]{:S(2)}, u32[]{:S(2)}) collective-permute-start(bf16[128,256]{1,0:T(8,128)(2,1)S(1)} %get-tuple-element.68), channel_id=1, source_target_pairs={{8,0},{16,8},{24,16},{9,1},{17,9},{25,17},{10,2},{18,10},{26,18},{... | collective-permute-start | bytes 196616 | tf_op jit(solution)/shard_map/ppermute | solution.py:413
  33.8 5.3 %collective-permute-done.8.high = bf16[128,256]{1,0:T(8,128)(2,1)S(1)} collective-permute-done((bf16[128,256]{1,0:T(8,128)(2,1)S(1)}, bf16[128,256]{1,0:T(8,128)(2,1)S(1)}, u32[]{:S(2)}, u32[]{:S(2)}) %collective-permute-start.8) | collective-permute-done | bytes 65568 | tf_op jit(solution)/shard_map/ppermute | solution.py:413
  39.1 2.0 %collective-permute-start.3 = (bf16[384,256]{1,0:T(8,128)(2,1)S(1)}, bf16[384,256]{1,0:T(8,128)(2,1)S(1)}, u32[]{:S(2)}, u32[]{:S(2)}) collective-permute-start(bf16[384,256]{1,0:T(8,128)(2,1)S(1)} %collective-permute-done.2.refs_3_), channel_id=1, source_target_pairs={{0,8},{8,16},{16,24},{24,0},{1,9},{9,17},{17,25},{25,1},{2,10},{10... | collective-permute-start | bytes 589832 | tf_op jit(solution)/shard_map/ppermute | solution.py:421
  41.1 0.0 collective-permute-done.refs_2_
  41.1 1.8 %collective-permute-start.1 = (bf16[384,256]{1,0:T(8,128)(2,1)S(1)}, bf16[384,256]{1,0:T(8,128)(2,1)S(1)}, u32[]{:S(2)}, u32[]{:S(2)}) collective-permute-start(bf16[384,256]{1,0:T(8,128)(2,1)S(1)} %collective-permute-done.refs_2_), channel_id=1, source_target_pairs={{8,0},{16,8},{24,16},{0,24},{9,1},{17,9},{25,17},{1,25},{10,2},{18... | collective-permute-start | bytes 589832 | tf_op jit(solution)/shard_map/ppermute | solution.py:421
  42.9 0.0 copy-done
  42.9 2.1 %banded.1 = (bf16[384,256]{1,0:T(8,128)(2,1)S(1)}, bf16[384,256]{1,0:T(8,128)(2,1)S(1)}) custom-call(f32[1,2]{1,0:T(1,128)S(1)} %bitcast.4, bf16[768,256]{1,0:T(8,128)(2,1)S(1)} %get-tuple-element.65.lq, bf16[768,256]{1,0:T(8,128)(2,1)S(1)} %get-tuple-element.66.lkv, bf16[128,256]{1,0:T(8,128)(2,1)S(1)} %collective-permute-done.7.low, ...), custom_call_target="tpu_custom_call" | custom-call | flops 181193936 | tf_op jit(solution)/shard_map/banded/pallas_call | solution.py:423
  45.0 0.0 collective-permute-done.4.refs_1_
  45.0 0.1 collective-permute-start.9
  45.1 1.9 %shard_map.146 = (f32[1536,128]{1,0:T(8,128)S(1)}, f32[1536,256]{1,0:T(8,128)S(1)}) custom-call(bf16[1536,128]{1,0:T(8,128)(2,1)S(1)} %get-tuple-element.54.refs_0_.q, bf16[384,256]{1,0:T(8,128)(2,1)S(1)} %collective-permute-done.4.refs_1_, bf16[384,256]{1,0:T(8,128)(2,1)S(1)} %collective-permute-done.refs_2_, f32[1536,128]{1,0:T(8,128)S(1)} %get-tuple-element.57.refs_3_, ...), custom_call_target="tpu_custom_call" | custom-call | flops 362387872 | tf_op jit(solution)/shard_map/pallas_call | solution.py:289
  47.0 1.2 %collective-permute-done.3.refs_1_ = bf16[384,256]{1,0:T(8,128)(2,1)S(1)} collective-permute-done((bf16[384,256]{1,0:T(8,128)(2,1)S(1)}, bf16[384,256]{1,0:T(8,128)(2,1)S(1)}, u32[]{:S(2)}, u32[]{:S(2)}) %collective-permute-start.3) | collective-permute-done | bytes 196640 | tf_op jit(solution)/shard_map/ppermute | solution.py:421
  48.2 1.6 %shard_map.147 = (f32[1536,128]{1,0:T(8,128)S(1)}, f32[1536,256]{1,0:T(8,128)S(1)}) custom-call(bf16[1536,128]{1,0:T(8,128)(2,1)S(1)} %get-tuple-element.54.refs_0_.q, bf16[384,256]{1,0:T(8,128)(2,1)S(1)} %collective-permute-done.3.refs_1_, f32[1536,128]{1,0:T(8,128)S(1)} %get-tuple-element.59.refs_2_, f32[1536,256]{1,0:T(8,128)S(1)} %get-tuple-element.60.refs_3_), custom_call_target="tpu_custom_call" | custom-call | flops 181193936 | tf_op jit(solution)/shard_map/pallas_call | solution.py:289
  49.8 0.1 collective-permute-done.1.kv
  49.9 0.6 shard_map.151
  50.5 0.1 collective-permute-start.13
  50.6 0.0 collective-permute-done.9.lother
  50.6 0.0 collective-permute-done.11.lw_other
  50.6 0.6 early.1
  51.2 0.6 collective-permute-done.13.other
  51.8 0.0 collective-permute-done.10.w_other
  51.8 0.3 pass_on.1
  52.1 1.5 %collective-permute-start.14 = (bf16[96,2048]{1,0:T(8,128)(2,1)S(1)}, bf16[96,2048]{1,0:T(8,128)(2,1)S(1)}, u32[]{:S(2)}, u32[]{:S(2)}) collective-permute-start(bf16[96,2048]{1,0:T(8,128)(2,1)S(1)} %pass_on.1), channel_id=1, source_target_pairs={{0,2},{1,5},{2,0},{3,7},{4,6},{5,1},{6,4},{7,3},{8,10},{9,13},{10,... | collective-permute-start | bytes 1179656 | tf_op jit(solution)/shard_map/ppermute | solution.py:462
  53.7 1.4 %shard_map.148 = (bf16[288,256]{1,0:T(8,128)(2,1)S(1)}, bf16[288,256]{1,0:T(8,128)(2,1)S(1)}) custom-call(bf16[1536,128]{1,0:T(8,128)(2,1)S(1)} %get-tuple-element.54.refs_0_.q, bf16[384,256]{1,0:T(8,128)(2,1)S(1)} %collective-permute-done.1.kv, f32[1536,128]{1,0:T(8,128)S(1)} %get-tuple-element.61.m_in, f32[1536,256]{1,0:T(8,128)S(1)} %get-tuple-element.62.acc_in), custom_call_target="tpu_custom_call" | custom-call | flops 135895456 | tf_op jit(solution)/shard_map/pallas_call | solution.py:304
  55.0 0.1 collective-permute-start.6
  55.1 1.4 %collective-permute-done.6.other = bf16[288,256]{1,0:T(8,128)(2,1)S(1)} collective-permute-done((bf16[288,256]{1,0:T(8,128)(2,1)S(1)}, bf16[288,256]{1,0:T(8,128)(2,1)S(1)}, u32[]{:S(2)}, u32[]{:S(2)}) %collective-permute-start.6) | collective-permute-done | bytes 147488 | tf_op jit(solution)/shard_map/ppermute | solution.py:441
  56.5 0.8 %shard_map.150 = bf16[96,2048]{1,0:T(8,128)(2,1)S(1)} custom-call(bf16[288,256]{1,0:T(8,128)(2,1)S(1)} %get-tuple-element.63.keep, bf16[288,256]{1,0:T(8,128)(2,1)S(1)} %collective-permute-done.6.other, bf16[384,256]{1,0:T(8,128)(2,1)S(1)} %get-tuple-element.69.lkeep, bf16[384,256]{1,0:T(8,128)(2,1)S(1)} %collective-permute-done.9.lother, ...), custom_call_target="tpu_custom_call" | custom-call | flops 120795952 | bytes 4194304 | tf_op jit(solution)/shard_map/pallas_call | solution.py:317
  57.3 1.1 %collective-permute-start.12 = (bf16[96,2048]{1,0:T(8,128)(2,1)S(1)}, bf16[96,2048]{1,0:T(8,128)(2,1)S(1)}, u32[]{:S(2)}, u32[]{:S(2)}) collective-permute-start(bf16[96,2048]{1,0:T(8,128)(2,1)S(1)} %shard_map.150), channel_id=1, source_target_pairs={{0,2},{1,5},{2,0},{3,7},{4,6},{5,1},{6,4},{7,3},{8,10},{9,13},{10,... | collective-permute-start | bytes 1179656 | tf_op jit(solution)/shard_map/ppermute | solution.py:465
  58.4 1.4 %shard_map.149 = (f32[96,2048]{1,0:T(8,128)S(1)}, f32[96,2048]{1,0:T(8,128)S(1)}) custom-call(bf16[288,256]{1,0:T(8,128)(2,1)S(1)} %get-tuple-element.63.keep, bf16[288,256]{1,0:T(8,128)(2,1)S(1)} %collective-permute-done.6.other, bf16[384,256]{1,0:T(8,128)(2,1)S(1)} %get-tuple-element.69.lkeep, bf16[384,256]{1,0:T(8,128)(2,1)S(1)} %collective-permute-done.9.lother, ...), custom_call_target="tpu_custom_call" | custom-call | flops 241591904 | bytes 4194304 | tf_op jit(solution)/shard_map/pallas_call | solution.py:317
  59.8 0.1 collective-permute-done.14
  59.9 0.1 add_convert_fusion.1
  60.0 1.6 %collective-permute-start.15 = (bf16[96,2048]{1,0:T(8,128)(2,1)S(1)}, bf16[96,2048]{1,0:T(8,128)(2,1)S(1)}, u32[]{:S(2)}, u32[]{:S(2)}) collective-permute-start(bf16[96,2048]{1,0:T(8,128)(2,1)S(1)} %add_convert_fusion.1), channel_id=1, source_target_pairs={{0,4},{1,3},{2,6},{3,1},{4,0},{5,7},{6,2},{7,5},{8,12},{9,11},{10,... | collective-permute-start | bytes 1179656 | tf_op jit(solution)/shard_map/ppermute | solution.py:466
  61.6 5.7 %collective-permute-done.12 = bf16[96,2048]{1,0:T(8,128)(2,1)S(1)} collective-permute-done((bf16[96,2048]{1,0:T(8,128)(2,1)S(1)}, bf16[96,2048]{1,0:T(8,128)(2,1)S(1)}, u32[]{:S(2)}, u32[]{:S(2)}) %collective-permute-start.12) | collective-permute-done | bytes 393248 | tf_op jit(solution)/shard_map/ppermute | solution.py:465
  67.3 1.2 %collective-permute-done.15 = bf16[96,2048]{1,0:T(8,128)(2,1)S(1)} collective-permute-done((bf16[96,2048]{1,0:T(8,128)(2,1)S(1)}, bf16[96,2048]{1,0:T(8,128)(2,1)S(1)}, u32[]{:S(2)}, u32[]{:S(2)}) %collective-permute-start.15) | collective-permute-done | bytes 393248 | tf_op jit(solution)/shard_map/ppermute | solution.py:466
  68.5 0.9 %add_convert_fusion = bf16[96,2048]{1,0:T(8,128)(2,1)} fusion(bf16[96,2048]{1,0:T(8,128)(2,1)S(1)} %collective-permute-done.15, f32[96,2048]{1,0:T(8,128)S(1)} %get-tuple-element.73, bf16[96,2048]{1,0:T(8,128)(2,1)S(1)} %collective-permute-done.12), kind=kLoop, calls=%fused_computation | loop fusion | flops 983040 | bytes 1966080 | tf_op jit(solution)/shard_map/convert_element_type | solution.py:468
  (1 shorter events, 0.0 us)
Async XLA Ops:
  2.7 10.9 %collective-permute-start.2 = (bf16[384,256]{1,0:T(8,128)(2,1)S(1)}, bf16[384,256]{1,0:T(8,128)(2,1)S(1)}, u32[]{:S(2)}, u32[]{:S(2)}) collective-permute-start(bf16[384,256]{1,0:T(8,128)(2,1)S(1)} %get-tuple-element.56.refs_1_), channel_id=1, source_target_pairs={{0,8},{8,16},{16,24},{24,0},{1,9},{9,17},{17,25},{25,1},{2,10},{10... | collective-permute-start | bytes 589832 | tf_op jit(solution)/shard_map/ppermute | solution.py:385
  5.8 10.6 %collective-permute-start.5 = (bf16[384,256]{1,0:T(8,128)(2,1)S(1)}, bf16[384,256]{1,0:T(8,128)(2,1)S(1)}, u32[]{:S(2)}, u32[]{:S(2)}) collective-permute-start(bf16[384,256]{1,0:T(8,128)(2,1)S(1)} %get-tuple-element.56.refs_1_), channel_id=1, source_target_pairs={{8,0},{16,8},{24,16},{0,24},{9,1},{17,9},{25,17},{1,25},{10,2},{18... | collective-permute-start | bytes 589832 | tf_op jit(solution)/shard_map/ppermute | solution.py:386
  16.3 26.6 %copy-start = (f32[2]{0:T(128)S(1)}, f32[2]{0:T(128)}, u32[]{:S(2)}) copy-start(f32[2]{0:T(128)} %param.25) | copy-start | bytes 28
  19.5 31.1 %collective-permute-start.11 = (bf16[256,2048]{1,0:T(8,128)(2,1)S(1)}, bf16[256,2048]{1,0:T(8,128)(2,1)S(1)}, u32[]{:S(2)}, u32[]{:S(2)}) collective-permute-start(bf16[256,2048]{1,0:T(8,128)(2,1)S(1)} %get-tuple-element.72.lw), channel_id=1, source_target_pairs={{0,1},{1,0},{2,3},{3,2},{4,5},{5,4},{6,7},{7,6},{8,9},{9,8},{10,11... | collective-permute-start | bytes 3145736 | tf_op jit(solution)/shard_map/ppermute | solution.py:416
  19.6 32.2 %collective-permute-start.10 = (bf16[256,2048]{1,0:T(8,128)(2,1)S(1)}, bf16[256,2048]{1,0:T(8,128)(2,1)S(1)}, u32[]{:S(2)}, u32[]{:S(2)}) collective-permute-start(bf16[256,2048]{1,0:T(8,128)(2,1)S(1)} %get-tuple-element.71.w), channel_id=1, source_target_pairs={{0,1},{1,0},{2,3},{3,2},{4,5},{5,4},{6,7},{7,6},{8,9},{9,8},{10,11... | collective-permute-start | bytes 3145736 | tf_op jit(solution)/shard_map/ppermute | solution.py:415
  20.1 21.0 %collective-permute-start = (bf16[384,256]{1,0:T(8,128)(2,1)S(1)}, bf16[384,256]{1,0:T(8,128)(2,1)S(1)}, u32[]{:S(2)}, u32[]{:S(2)}) collective-permute-start(bf16[384,256]{1,0:T(8,128)(2,1)S(1)} %get-tuple-element.55.refs_2_), channel_id=1, source_target_pairs={{8,0},{16,8},{24,16},{0,24},{9,1},{17,9},{25,17},{1,25},{10,2},{18... | collective-permute-start | bytes 589832 | tf_op jit(solution)/shard_map/ppermute | solution.py:388
  22.4 22.6 %collective-permute-start.4 = (bf16[384,256]{1,0:T(8,128)(2,1)S(1)}, bf16[384,256]{1,0:T(8,128)(2,1)S(1)}, u32[]{:S(2)}, u32[]{:S(2)}) collective-permute-start(bf16[384,256]{1,0:T(8,128)(2,1)S(1)} %get-tuple-element.55.refs_2_), channel_id=1, source_target_pairs={{0,8},{8,16},{16,24},{24,0},{1,9},{9,17},{17,25},{25,1},{2,10},{10... | collective-permute-start | bytes 589832 | tf_op jit(solution)/shard_map/ppermute | solution.py:387
  22.4 10.1 %collective-permute-start.7 = (bf16[128,256]{1,0:T(8,128)(2,1)S(1)}, bf16[128,256]{1,0:T(8,128)(2,1)S(1)}, u32[]{:S(2)}, u32[]{:S(2)}) collective-permute-start(bf16[128,256]{1,0:T(8,128)(2,1)S(1)} %get-tuple-element.67), channel_id=1, source_target_pairs={{0,8},{8,16},{16,24},{1,9},{9,17},{17,25},{2,10},{10,18},{18,26},{... | collective-permute-start | bytes 196616 | tf_op jit(solution)/shard_map/ppermute | solution.py:412
  32.5 6.6 %collective-permute-start.8 = (bf16[128,256]{1,0:T(8,128)(2,1)S(1)}, bf16[128,256]{1,0:T(8,128)(2,1)S(1)}, u32[]{:S(2)}, u32[]{:S(2)}) collective-permute-start(bf16[128,256]{1,0:T(8,128)(2,1)S(1)} %get-tuple-element.68), channel_id=1, source_target_pairs={{8,0},{16,8},{24,16},{9,1},{17,9},{25,17},{10,2},{18,10},{26,18},{... | collective-permute-start | bytes 196616 | tf_op jit(solution)/shard_map/ppermute | solution.py:413
  39.1 9.1 %collective-permute-start.3 = (bf16[384,256]{1,0:T(8,128)(2,1)S(1)}, bf16[384,256]{1,0:T(8,128)(2,1)S(1)}, u32[]{:S(2)}, u32[]{:S(2)}) collective-permute-start(bf16[384,256]{1,0:T(8,128)(2,1)S(1)} %collective-permute-done.2.refs_3_), channel_id=1, source_target_pairs={{0,8},{8,16},{16,24},{24,0},{1,9},{9,17},{17,25},{25,1},{2,10},{10... | collective-permute-start | bytes 589832 | tf_op jit(solution)/shard_map/ppermute | solution.py:421
  41.1 8.8 %collective-permute-start.1 = (bf16[384,256]{1,0:T(8,128)(2,1)S(1)}, bf16[384,256]{1,0:T(8,128)(2,1)S(1)}, u32[]{:S(2)}, u32[]{:S(2)}) collective-permute-start(bf16[384,256]{1,0:T(8,128)(2,1)S(1)} %collective-permute-done.refs_2_), channel_id=1, source_target_pairs={{8,0},{16,8},{24,16},{0,24},{9,1},{17,9},{25,17},{1,25},{10,2},{18... | collective-permute-start | bytes 589832 | tf_op jit(solution)/shard_map/ppermute | solution.py:421
  45.0 5.6 %collective-permute-start.9 = (bf16[384,256]{1,0:T(8,128)(2,1)S(1)}, bf16[384,256]{1,0:T(8,128)(2,1)S(1)}, u32[]{:S(2)}, u32[]{:S(2)}) collective-permute-start(bf16[384,256]{1,0:T(8,128)(2,1)S(1)} %get-tuple-element.70), channel_id=1, source_target_pairs={{0,1},{1,0},{2,3},{3,2},{4,5},{5,4},{6,7},{7,6},{8,9},{9,8},{10,11... | collective-permute-start | bytes 589832 | tf_op jit(solution)/shard_map/ppermute | solution.py:433
  50.5 1.3 %collective-permute-start.13 = (bf16[96,256]{1,0:T(8,128)(2,1)S(1)}, bf16[96,256]{1,0:T(8,128)(2,1)S(1)}, u32[]{:S(2)}, u32[]{:S(2)}) collective-permute-start(bf16[96,256]{1,0:T(8,128)(2,1)S(1)} %get-tuple-element.76), channel_id=1, source_target_pairs={{0,1},{1,0},{2,3},{3,2},{4,5},{5,4},{6,7},{7,6},{8,9},{9,8},{10,11... | collective-permute-start | bytes 147464 | tf_op jit(solution)/shard_map/ppermute | solution.py:439
  52.1 7.8 %collective-permute-start.14 = (bf16[96,2048]{1,0:T(8,128)(2,1)S(1)}, bf16[96,2048]{1,0:T(8,128)(2,1)S(1)}, u32[]{:S(2)}, u32[]{:S(2)}) collective-permute-start(bf16[96,2048]{1,0:T(8,128)(2,1)S(1)} %pass_on.1), channel_id=1, source_target_pairs={{0,2},{1,5},{2,0},{3,7},{4,6},{5,1},{6,4},{7,3},{8,10},{9,13},{10,... | collective-permute-start | bytes 1179656 | tf_op jit(solution)/shard_map/ppermute | solution.py:462
  55.0 1.4 %collective-permute-start.6 = (bf16[288,256]{1,0:T(8,128)(2,1)S(1)}, bf16[288,256]{1,0:T(8,128)(2,1)S(1)}, u32[]{:S(2)}, u32[]{:S(2)}) collective-permute-start(bf16[288,256]{1,0:T(8,128)(2,1)S(1)} %get-tuple-element.64), channel_id=1, source_target_pairs={{0,1},{1,0},{2,3},{3,2},{4,5},{5,4},{6,7},{7,6},{8,9},{9,8},{10,11... | collective-permute-start | bytes 442376 | tf_op jit(solution)/shard_map/ppermute | solution.py:441
  57.3 10.0 %collective-permute-start.12 = (bf16[96,2048]{1,0:T(8,128)(2,1)S(1)}, bf16[96,2048]{1,0:T(8,128)(2,1)S(1)}, u32[]{:S(2)}, u32[]{:S(2)}) collective-permute-start(bf16[96,2048]{1,0:T(8,128)(2,1)S(1)} %shard_map.150), channel_id=1, source_target_pairs={{0,2},{1,5},{2,0},{3,7},{4,6},{5,1},{6,4},{7,3},{8,10},{9,13},{10,... | collective-permute-start | bytes 1179656 | tf_op jit(solution)/shard_map/ppermute | solution.py:465
  60.0 8.5 %collective-permute-start.15 = (bf16[96,2048]{1,0:T(8,128)(2,1)S(1)}, bf16[96,2048]{1,0:T(8,128)(2,1)S(1)}, u32[]{:S(2)}, u32[]{:S(2)}) collective-permute-start(bf16[96,2048]{1,0:T(8,128)(2,1)S(1)} %add_convert_fusion.1), channel_id=1, source_target_pairs={{0,4},{1,3},{2,6},{3,1},{4,0},{5,7},{6,2},{7,5},{8,12},{9,11},{10,... | collective-permute-start | bytes 1179656 | tf_op jit(solution)/shard_map/ppermute | solution.py:466
